TPU v7x, 32 devices: a whole 2x2x4 slice. The times are simulated.
32 devices in a mesh: grp: 2 (over x), ep: 8 (over z, y), tp: 2 (over core).
Axes of the slice: x: 2, y: 2, z: 4, core: 2. Of those that a mesh axis runs over, the one named last changes fastest.
Arguments:
- tokens: bfloat16 [512, 2048], P(('grp', 'ep')), parts along dimension 0, may hold values from -6 to 6
- norm_gain: float32 [2048], replicated, may hold values from 0.1 to 1.9
- group_prob: float32 [512], P(('grp', 'ep')), parts along dimension 0, may hold values from 0.5 to 1
- route_logits: float32 [512, 4], P(('grp', 'ep')), parts along dimension 0, may hold values from -6 to 6
- expert_ids: int32 [512, 4], P(('grp', 'ep')), parts along dimension 0, may hold values from 0 to 7, as said below
- w_gate: bfloat16 [8, 2048, 512], P('ep', None, 'tp'), may hold values from -0.125 to 0.125
- w_up: bfloat16 [8, 2048, 512], P('ep', None, 'tp'), may hold values from -0.125 to 0.125
- w_down: bfloat16 [8, 512, 2048], P('ep', 'tp'), may hold values from -0.25 to 0.25
Outputs:
- mixed: bfloat16 [512, 2048], P(('grp', 'ep')), parts along dimension 0
There are 2 independent parts, one for each index of `grp`. A program takes and returns all parts, laid end to end along the dimension named above; an argument that names none is the same for every part. Nothing has to cross between parts.
Inputs may be any that keep to these rules, and one draw needn't show every extreme that they name: `expert_ids`: each token names 4 different experts, all inside one group of 4 consecutive experts. Of the 32 tokens of one index of ep, exactly 16 lie in each group, so at most 16 of them name any one expert; in every draw some expert is named by 16 tokens of every index of ep.
All inputs are finite; a program needn't handle non-finite values.
Results may differ from a plain program's by a relative error of at most 0.0077.
Values may be sent and summed in bfloat16 or wider, within the bound.
A program may use at most 64 MiB of HBM per device.

v0:
```python
import functools

import jax
import jax.numpy as jnp
from jax import lax
from jax.experimental import pallas as pl
from jax.experimental.pallas import tpu as pltpu
from jax.sharding import PartitionSpec as P

GROUPS = 2
MESH = pl.DeviceIdType.MESH


def kernel(
    width, n_tp,
    tok_hbm, gain_hbm, prob_hbm, logit_hbm, ids_hbm, wg_hbm, wu_hbm, wd_hbm,
    out_ref,
    tok, gain, prob, logit, ids, wg, wu, wd, send, recv, outs, back, mixed,
    in_sem, wl_sem, ws_sem, wr_sem, ds_sem, dr_sem, bs_sem, br_sem, ms_sem, mr_sem,
):
    e = lax.axis_index("ep")
    q = lax.axis_index("tp")
    sib = n_tp - 1 - q
    gs = width // GROUPS
    nsrc = width // n_tp
    hb = nsrc // GROUPS
    count, dmodel = tok.shape
    cap = count // GROUPS
    topk = ids.shape[0]
    block = e // gs
    mine = (block == q) & (e % n_tp == q)

    smalls = [
        pltpu.make_async_copy(src, dst, in_sem.at[i])
        for i, (src, dst) in enumerate(
            [(tok_hbm, tok), (gain_hbm, gain), (prob_hbm, prob), (logit_hbm, logit), (ids_hbm, ids)]
        )
    ]
    for c in smalls:
        c.start()
    weights = [(wg_hbm, wg), (wu_hbm, wu), (wd_hbm, wd)]
    locals_ = [
        pltpu.make_async_copy(src.at[0], dst.at[q], wl_sem.at[i]) for i, (src, dst) in enumerate(weights)
    ]
    for c in locals_:
        c.start()

    barrier = pltpu.get_barrier_semaphore()
    pl.semaphore_signal(barrier, inc=1, device_id={"tp": sib}, device_id_type=MESH)
    for j in range(gs):
        dest = q * gs + j

        @pl.when(jnp.logical_not(mine & (dest == e)))
        def _():
            pl.semaphore_signal(
                barrier, inc=1, device_id={"ep": dest, "tp": e % n_tp}, device_id_type=MESH
            )

    for i in range(nsrc):
        src = i * n_tp + q

        @pl.when(jnp.logical_not(mine & (src == e)))
        def _():
            pl.semaphore_signal(
                barrier, inc=1, device_id={"ep": src, "tp": block}, device_id_type=MESH
            )

    for c in smalls:
        c.wait()
    values = tok[...].astype(jnp.float32)
    scale = lax.rsqrt(jnp.mean(values * values, axis=-1, keepdims=True) + 1e-06)
    normed = (values * scale * gain[...]).astype(jnp.bfloat16)
    idv = ids[...]
    first = idv[0:1, :]
    grow = jnp.zeros((1, count), jnp.float32)
    for g in range(1, GROUPS):
        grow = grow + jnp.where(first >= g * gs, 1.0, 0.0)
    t_row = lax.broadcasted_iota(jnp.int32, (count, count), 0)
    t_col = lax.broadcasted_iota(jnp.int32, (count, count), 1)
    gfull = jnp.broadcast_to(grow, (count, count))
    gcol = jnp.sum(jnp.where(t_row == t_col, gfull, 0.0), axis=1, keepdims=True)
    same = jnp.where(gfull == gcol, 1.0, 0.0)
    pos_row = jnp.sum(jnp.where(t_row < t_col, same, 0.0), axis=0, keepdims=True)
    pos_col = jnp.sum(jnp.where(t_col < t_row, same, 0.0), axis=1, keepdims=True)
    qf = q.astype(jnp.float32)
    r_io = lax.broadcasted_iota(jnp.int32, (cap, count), 0).astype(jnp.float32)
    place = jnp.where((pos_row == r_io) & (grow == qf), 1.0, 0.0)
    send[...] = jnp.dot(
        place.astype(jnp.bfloat16), normed, preferred_element_type=jnp.float32
    ).astype(jnp.bfloat16)

    @pl.when(mine)
    def _():
        recv[e // n_tp] = send[...]

    wait_n = jnp.where(mine, gs + nsrc - 1, gs + nsrc + 1)
    pl.semaphore_wait(barrier, wait_n)

    def dispatch(j):
        dest = q * gs + j
        return dest, pltpu.make_async_remote_copy(
            src_ref=send,
            dst_ref=recv.at[e // n_tp],
            send_sem=ds_sem.at[j],
            recv_sem=dr_sem.at[e // n_tp],
            device_id={"ep": dest, "tp": e % n_tp},
            device_id_type=MESH,
        )

    for j in range(gs):
        dest, copy = dispatch(j)

        @pl.when(jnp.logical_not(mine & (dest == e)))
        def _():
            copy.start()

    swaps = [
        pltpu.make_async_remote_copy(
            src_ref=src.at[0],
            dst_ref=dst.at[q],
            send_sem=ws_sem.at[i],
            recv_sem=wr_sem.at[i],
            device_id={"tp": sib},
            device_id_type=MESH,
        )
        for i, (src, dst) in enumerate(weights)
    ]
    for c in swaps:
        c.start()

    expw = jnp.exp(logit[...])
    route = prob[...] * expw / jnp.sum(expw, axis=0, keepdims=True)
    expert = lax.broadcasted_iota(jnp.int32, (128, count), 0) + q * gs
    wtok = jnp.zeros((128, count), jnp.float32)
    for k in range(topk):
        wtok = wtok + jnp.where(idv[k : k + 1, :] == expert, route[k : k + 1, :], 0.0)
    wslot = lax.dot_general(
        place, wtok, (((1,), (1,)), ((), ())),
        precision=lax.Precision.HIGHEST, preferred_element_type=jnp.float32,
    )
    s_io = lax.broadcasted_iota(jnp.int32, (count, count), 1).astype(jnp.float32)
    unplace = jnp.where(s_io == gcol * cap + pos_col, 1.0, 0.0).astype(jnp.bfloat16)

    def give(i):
        home = i * n_tp + q
        return home, pltpu.make_async_remote_copy(
            src_ref=outs.at[i],
            dst_ref=back.at[e % gs],
            send_sem=bs_sem.at[i],
            recv_sem=br_sem.at[e % gs],
            device_id={"ep": home, "tp": block},
            device_id_type=MESH,
        )

    for c in locals_:
        c.wait()
    for step in range(GROUPS):
        b = lax.rem(block + step, GROUPS)
        for i in range(hb):
            slot = b * hb + i

            @pl.when(jnp.logical_not(mine & (slot * n_tp + q == e)))
            def _():
                pltpu.make_async_remote_copy(
                    src_ref=send,
                    dst_ref=recv.at[slot],
                    send_sem=ds_sem.at[0],
                    recv_sem=dr_sem.at[slot],
                    device_id={"tp": sib},
                    device_id_type=MESH,
                ).wait_recv()

        def arrived(i):
            if step == 0:
                src, dst = weights[i]
                pltpu.make_async_remote_copy(
                    src_ref=src.at[0],
                    dst_ref=dst.at[sib],
                    send_sem=ws_sem.at[i],
                    recv_sem=wr_sem.at[i],
                    device_id={"tp": sib},
                    device_id_type=MESH,
                ).wait_recv()

        x = recv[pl.ds(b * hb, hb)].reshape(hb * cap, dmodel)
        arrived(0)
        gates = [jnp.dot(x, wg[h], preferred_element_type=jnp.float32) for h in range(n_tp)]
        arrived(1)
        ups = [jnp.dot(x, wu[h], preferred_element_type=jnp.float32) for h in range(n_tp)]
        acts = [((g / (1.0 + jnp.exp(-g))) * u).astype(jnp.bfloat16) for g, u in zip(gates, ups)]
        arrived(2)
        total = jnp.dot(acts[0], wd[0], preferred_element_type=jnp.float32)
        for h in range(1, n_tp):
            total = total + jnp.dot(acts[h], wd[h], preferred_element_type=jnp.float32)
        outs[pl.ds(b * hb, hb)] = total.astype(jnp.bfloat16).reshape(hb, cap, dmodel)
        for i in range(hb):
            slot = b * hb + i
            home, copy = give(slot)

            @pl.when(jnp.logical_not(mine & (home == e)))
            def _():
                copy.start()

            @pl.when(mine & (home == e))
            def _():
                back[e % gs] = outs[slot]

    acc = jnp.zeros((cap, dmodel), jnp.float32)
    for j in range(gs):

        @pl.when(jnp.logical_not(mine & (q * gs + j == e)))
        def _():
            pltpu.make_async_remote_copy(
                src_ref=outs.at[0],
                dst_ref=back.at[j],
                send_sem=bs_sem.at[0],
                recv_sem=br_sem.at[j],
                device_id={"tp": sib},
                device_id_type=MESH,
            ).wait_recv()

        acc = acc + wslot[:, j : j + 1] * back[j].astype(jnp.float32)
    mixed[q] = acc.astype(jnp.bfloat16)
    swap = pltpu.make_async_remote_copy(
        src_ref=mixed.at[q],
        dst_ref=mixed.at[q],
        send_sem=ms_sem,
        recv_sem=mr_sem,
        device_id={"tp": sib},
        device_id_type=MESH,
    )
    swap.start()

    for j in range(gs):
        dest, copy = dispatch(j)

        @pl.when(jnp.logical_not(mine & (dest == e)))
        def _():
            copy.wait_send()

    for c in swaps:
        c.wait_send()
    for i in range(nsrc):
        home, copy = give(i)

        @pl.when(jnp.logical_not(mine & (home == e)))
        def _():
            copy.wait_send()

    pltpu.make_async_remote_copy(
        src_ref=mixed.at[q],
        dst_ref=mixed.at[sib],
        send_sem=ms_sem,
        recv_sem=mr_sem,
        device_id={"tp": sib},
        device_id_type=MESH,
    ).wait_recv()
    swap.wait_send()
    slots = mixed[...].reshape(count, dmodel)
    out_ref[...] = jnp.dot(unplace, slots, preferred_element_type=jnp.float32).astype(jnp.bfloat16)


def shards(tokens, norm_gain, group_prob, route_logits, expert_ids, w_gate, w_up, w_down):
    width = lax.axis_size("ep")
    n_tp = lax.axis_size("tp")
    count, dmodel = tokens.shape
    topk = expert_ids.shape[1]
    ff = w_gate.shape[2]
    cap = count // GROUPS
    gs = width // GROUPS
    nsrc = width // n_tp
    hbm = pl.BlockSpec(memory_space=pltpu.HBM)
    bf, f32 = jnp.bfloat16, jnp.float32
    dma = pltpu.SemaphoreType.DMA
    return pl.pallas_call(
        functools.partial(kernel, width, n_tp),
        out_shape=pltpu.VMEM((count, dmodel), bf),
        in_specs=[hbm] * 8,
        out_specs=pl.BlockSpec(memory_space=pltpu.VMEM),
        scratch_shapes=[
            pltpu.VMEM((count, dmodel), bf),
            pltpu.VMEM((1, dmodel), f32),
            pltpu.VMEM((1, count), f32),
            pltpu.VMEM((topk, count), f32),
            pltpu.VMEM((topk, count), jnp.int32),
            pltpu.VMEM((n_tp, dmodel, ff), bf),
            pltpu.VMEM((n_tp, dmodel, ff), bf),
            pltpu.VMEM((n_tp, ff, dmodel), bf),
            pltpu.VMEM((cap, dmodel), bf),
            pltpu.VMEM((nsrc, cap, dmodel), bf),
            pltpu.VMEM((nsrc, cap, dmodel), bf),
            pltpu.VMEM((gs, cap, dmodel), bf),
            pltpu.VMEM((n_tp, cap, dmodel), bf),
            dma((5,)), dma((3,)), dma((3,)), dma((3,)),
            dma((gs,)), dma((nsrc,)), dma((nsrc,)), dma((gs,)),
            dma, dma,
        ],
        compiler_params=pltpu.CompilerParams(collective_id=0, has_side_effects=True),
        name="expert_mixture",
    )(
        tokens, norm_gain.reshape(1, dmodel), group_prob.reshape(1, count), route_logits.T,
        expert_ids.T, w_gate, w_up, w_down,
    )


def solution(mesh):
    in_specs = (
        P(("grp", "ep"), None),
        P(),
        P(("grp", "ep")),
        P(("grp", "ep"), None),
        P(("grp", "ep"), None),
        P("ep", None, "tp"),
        P("ep", None, "tp"),
        P("ep", "tp", None),
    )
    out_specs = P(("grp", "ep"), None)
    return jax.shard_map(shards, mesh=mesh, in_specs=in_specs, out_specs=out_specs, check_vma=False)
```

profile of v0, /device:TPU:0, one launch (start us, length us, event | category | flops | bytes accessed | tf_op | source)
XLA Modules:
  0.0 22.0 jit_solution(17251041690741424203)
XLA Ops:
  0.0 21.4 %expert_mixture.1 = bf16[32,2048]{1,0:T(8,128)(2,1)S(1)} custom-call(bf16[32,2048]{1,0:T(8,128)(2,1)} %tok_hbm.1, f32[1,2048]{1,0:T(1,128)} %bitcast.4, f32[1,32]{1,0:T(1,128)} %bitcast.7, f32[4,32]{1,0:T(4,128)} %bitcast.5, s32[4,32]{1,0:T(4,128)} %bitcast.6, bf16[1,2048,256]{2,1,0:T(8,128)(2,1)} %wg_hbm.1, bf16[1,2048,256]{2,1,0:T(8,128)(2,1)} %wu_hbm.1, ...), custom_call_target="tpu_custom_call" | custom-call | tf_op jit(solution)/shard_map/expert_mixture/pallas_call | solution.py:275
  21.4 0.7 %copy.10 = bf16[32,2048]{1,0:T(8,128)(2,1)} copy(bf16[32,2048]{1,0:T(8,128)(2,1)S(1)} %expert_mixture.1) | data formatting | bytes 262144
where the time goes:
time: 22.2 us; the launch traced here: 22 us
  Pallas kernels  21.4 us (96%)
  local copies, waits for them, and re-layouts  0.66 us (3%)
    pallas_call x1, Pallas kernels, shards(): pl.pallas_call(functools.partial(kernel, width, n_tp), out_shape=pltpu.VM...  21.4 us
    unnamed x1, local copies, waits for them, and re-layouts  0.66 us

commit v1 on v0

v1 whole, which is shorter than its diff:
```python
import functools

import jax
import jax.numpy as jnp
from jax import lax
from jax.experimental import pallas as pl
from jax.experimental.pallas import tpu as pltpu
from jax.sharding import PartitionSpec as P

GROUPS = 2
CHUNKS = 4
MESH = pl.DeviceIdType.MESH


def kernel(
    width, n_tp,
    tok_hbm, gain_hbm, prob_hbm, logit_hbm, ids_hbm, wg_hbm, wu_hbm, wd_hbm,
    out_ref,
    tok, gain, prob, logit, ids, wg, wu, wd, send, wsend, wroot, x, outs, back, red, mixed,
    in_sem, wl_sem, ws_sem, wr_sem, xs_sem, xr_sem, vs_sem, vr_sem,
    ds_sem, dr_sem, bs_sem, br_sem, cs_sem, cr_sem, ms_sem, mr_sem,
):
    e = lax.axis_index("ep")
    q = lax.axis_index("tp")
    sib = n_tp - 1 - q
    gs = width // GROUPS
    count, dmodel = tok.shape
    cap = count // GROUPS
    topk = ids.shape[0]
    block = e // gs
    local = e % gs
    base = block * gs
    partner = (e + gs) % width
    cross = q == n_tp - 1
    own = q != n_tp - 1
    group = (block + q) % GROUPS
    cw = dmodel // CHUNKS
    f32, bf = jnp.float32, jnp.bfloat16

    def cols(c):
        return pl.ds(c * cw, cw)

    def peer(j):
        return base + (local + j) % gs

    def remote(src, dst, ss, rs, **where):
        return pltpu.make_async_remote_copy(
            src_ref=src, dst_ref=dst, send_sem=ss, recv_sem=rs,
            device_id=where, device_id_type=MESH,
        )

    smalls = [
        pltpu.make_async_copy(src, dst, in_sem.at[i])
        for i, (src, dst) in enumerate(
            [(tok_hbm, tok), (gain_hbm, gain), (prob_hbm, prob), (logit_hbm, logit), (ids_hbm, ids)]
        )
    ]
    for c in smalls:
        c.start()
    weights = [(wg_hbm, wg), (wu_hbm, wu), (wd_hbm, wd)]
    loads = [
        pltpu.make_async_copy(src.at[0], dst.at[q], wl_sem.at[i]) for i, (src, dst) in enumerate(weights)
    ]
    for c in loads:
        c.start()

    barrier = pltpu.get_barrier_semaphore()

    @pl.when(cross)
    def _():
        pl.semaphore_signal(barrier, inc=1, device_id={"ep": partner}, device_id_type=MESH)

    for j in range(1, gs):
        pl.semaphore_signal(barrier, inc=1, device_id={"ep": peer(j)}, device_id_type=MESH)
    pl.semaphore_signal(barrier, inc=1, device_id={"tp": sib}, device_id_type=MESH)

    for c in smalls:
        c.wait()
    values = tok[...].astype(f32)
    scale = lax.rsqrt(jnp.mean(values * values, axis=-1, keepdims=True) + 1e-06)
    normed = (values * scale * gain[...]).astype(bf)
    idv = ids[...]
    first = idv[0:1, :]
    grow = jnp.zeros((1, count), f32)
    for g in range(1, GROUPS):
        grow = grow + jnp.where(first >= g * gs, 1.0, 0.0)
    t_row = lax.broadcasted_iota(jnp.int32, (count, count), 0)
    t_col = lax.broadcasted_iota(jnp.int32, (count, count), 1)
    gfull = jnp.broadcast_to(grow, (count, count))
    gcol = jnp.sum(jnp.where(t_row == t_col, gfull, 0.0), axis=1, keepdims=True)
    same = jnp.where(gfull == gcol, 1.0, 0.0)
    pos_row = jnp.sum(jnp.where(t_row < t_col, same, 0.0), axis=0, keepdims=True)
    pos_col = jnp.sum(jnp.where(t_col < t_row, same, 0.0), axis=1, keepdims=True)
    r_io = lax.broadcasted_iota(jnp.int32, (cap, count), 0).astype(f32)
    place = jnp.where((pos_row == r_io) & (grow == group.astype(f32)), 1.0, 0.0)
    rows = jnp.dot(place.astype(bf), normed, preferred_element_type=f32).astype(bf)

    @pl.when(cross)
    def _():
        send[...] = rows

    @pl.when(own)
    def _():
        x[0] = rows

    pl.semaphore_wait(barrier, jnp.where(cross, gs + 1, gs))

    def across(c):
        return remote(send.at[:, cols(c)], x.at[0, :, cols(c)], xs_sem.at[c], xr_sem.at[c], ep=partner)

    def spread(j, c):
        return remote(
            x.at[0, :, cols(c)], x.at[j, :, cols(c)], ds_sem.at[j, c], dr_sem.at[j, c], ep=peer(j)
        )

    @pl.when(cross)
    def _():
        for c in range(CHUNKS):
            across(c).start()

    @pl.when(own)
    def _():
        for c in range(CHUNKS):
            for j in range(1, gs):
                spread(j, c).start()

    def swap(i, c):
        ref = weights[i][1]
        part = ref.at[q, cols(c)] if i < 2 else ref.at[q, :, cols(c)]
        return remote(part, part, ws_sem.at[i, c], wr_sem.at[i, c], tp=sib)

    def swapped(i, c):
        ref = weights[i][1]
        part = ref.at[sib, cols(c)] if i < 2 else ref.at[sib, :, cols(c)]
        return remote(part, part, ws_sem.at[i, c], wr_sem.at[i, c], tp=sib)

    loads[0].wait()
    loads[1].wait()
    for c in range(CHUNKS):
        for i in range(2):
            swap(i, c).start()
    loads[2].wait()
    for c in range(CHUNKS):
        swap(2, c).start()

    expw = jnp.exp(logit[...])
    route = prob[...] * expw / jnp.sum(expw, axis=0, keepdims=True)
    k_io = lax.broadcasted_iota(jnp.int32, (128, count), 0)
    expert = jnp.where(k_io < gs, group * gs + lax.rem(k_io + local, gs), -1)
    wtok = jnp.zeros((128, count), f32)
    for k in range(topk):
        wtok = wtok + jnp.where(idv[k : k + 1, :] == expert, route[k : k + 1, :], 0.0)
    wslot = lax.dot_general(
        place, wtok, (((1,), (1,)), ((), ())),
        precision=lax.Precision.HIGHEST, preferred_element_type=f32,
    )

    def weights_across():
        return remote(wsend, wroot, vs_sem, vr_sem, ep=partner)

    @pl.when(cross)
    def _():
        wsend[...] = wslot
        weights_across().start()

    @pl.when(own)
    def _():
        wroot[...] = wslot

    s_io = lax.broadcasted_iota(jnp.int32, (count, count), 1).astype(f32)
    role = jnp.where(gcol == block.astype(f32), 0.0, 1.0)
    unplace = jnp.where(s_io == role * cap + pos_col, 1.0, 0.0).astype(bf)

    @pl.when(cross)
    def _():
        for c in range(CHUNKS):
            across(c).wait_recv()
            for j in range(1, gs):
                spread(j, c).start()

    gates = [jnp.zeros((gs * cap, wg.shape[2]), f32)] * n_tp
    ups = [jnp.zeros((gs * cap, wu.shape[2]), f32)] * n_tp
    for c in range(CHUNKS):
        for i in range(2):
            swapped(i, c).wait_recv()
        for j in range(1, gs):
            spread(j, c).wait_recv()
        xc = x[:, :, c * cw : (c + 1) * cw].reshape(gs * cap, cw)
        for h in range(n_tp):
            gates[h] = gates[h] + jnp.dot(xc, wg[h, c * cw : (c + 1) * cw], preferred_element_type=f32)
            ups[h] = ups[h] + jnp.dot(xc, wu[h, c * cw : (c + 1) * cw], preferred_element_type=f32)
    acts = [((g / (1.0 + jnp.exp(-g))) * u).astype(bf) for g, u in zip(gates, ups)]

    def give(j, c):
        return remote(
            outs.at[j, :, cols(c)], back.at[j, :, cols(c)], bs_sem.at[j, c], br_sem.at[j, c],
            ep=base + (local + gs - j) % gs,
        )

    for c in range(CHUNKS):
        swapped(2, c).wait_recv()
        total = jnp.dot(acts[0], wd[0, :, c * cw : (c + 1) * cw], preferred_element_type=f32)
        for h in range(1, n_tp):
            total = total + jnp.dot(acts[h], wd[h, :, c * cw : (c + 1) * cw], preferred_element_type=f32)
        outs[:, :, c * cw : (c + 1) * cw] = total.astype(bf).reshape(gs, cap, cw)
        for j in range(1, gs):
            give(j, c).start()

    def home(c):
        return remote(
            red.at[:, cols(c)], mixed.at[n_tp - 1, :, cols(c)], cs_sem.at[c], cr_sem.at[c], ep=partner
        )

    def share(c):
        part = mixed.at[q, :, cols(c)]
        return remote(part, part, ms_sem.at[c], mr_sem.at[c], tp=sib)

    def shared(c):
        part = mixed.at[sib, :, cols(c)]
        return remote(part, part, ms_sem.at[c], mr_sem.at[c], tp=sib)

    @pl.when(cross)
    def _():
        weights_across().wait_recv()

    wv = wroot[...]
    for c in range(CHUNKS):
        acc = wv[:, 0:1] * outs[0, :, c * cw : (c + 1) * cw].astype(f32)
        for j in range(1, gs):
            give(j, c).wait_recv()
            acc = acc + wv[:, j : j + 1] * back[j, :, c * cw : (c + 1) * cw].astype(f32)
        done = acc.astype(bf)

        @pl.when(cross)
        def _():
            red[:, c * cw : (c + 1) * cw] = done
            home(c).start()

        @pl.when(own)
        def _():
            mixed[0, :, c * cw : (c + 1) * cw] = done
            share(c).start()

    @pl.when(cross)
    def _():
        for c in range(CHUNKS):
            home(c).wait_recv()
            share(c).start()

    for c in range(CHUNKS):
        shared(c).wait_recv()
        slots = mixed[:, :, c * cw : (c + 1) * cw].reshape(count, cw)
        out_ref[:, c * cw : (c + 1) * cw] = jnp.dot(unplace, slots, preferred_element_type=f32).astype(bf)

    @pl.when(cross)
    def _():
        weights_across().wait_send()
        for c in range(CHUNKS):
            across(c).wait_send()
            home(c).wait_send()

    for c in range(CHUNKS):
        for i in range(3):
            swap(i, c).wait_send()
        for j in range(1, gs):
            spread(j, c).wait_send()
            give(j, c).wait_send()
        share(c).wait_send()


def shards(tokens, norm_gain, group_prob, route_logits, expert_ids, w_gate, w_up, w_down):
    width = lax.axis_size("ep")
    n_tp = lax.axis_size("tp")
    count, dmodel = tokens.shape
    topk = expert_ids.shape[1]
    ff = w_gate.shape[2]
    cap = count // GROUPS
    gs = width // GROUPS
    hbm = pl.BlockSpec(memory_space=pltpu.HBM)
    bf, f32 = jnp.bfloat16, jnp.float32
    dma = pltpu.SemaphoreType.DMA
    return pl.pallas_call(
        functools.partial(kernel, width, n_tp),
        out_shape=pltpu.VMEM((count, dmodel), bf),
        in_specs=[hbm] * 8,
        out_specs=pl.BlockSpec(memory_space=pltpu.VMEM),
        scratch_shapes=[
            pltpu.VMEM((count, dmodel), bf),
            pltpu.VMEM((1, dmodel), f32),
            pltpu.VMEM((1, count), f32),
            pltpu.VMEM((topk, count), f32),
            pltpu.VMEM((topk, count), jnp.int32),
            pltpu.VMEM((n_tp, dmodel, ff), bf),
            pltpu.VMEM((n_tp, dmodel, ff), bf),
            pltpu.VMEM((n_tp, ff, dmodel), bf),
            pltpu.VMEM((cap, dmodel), bf),
            pltpu.VMEM((cap, 128), f32),
            pltpu.VMEM((cap, 128), f32),
            pltpu.VMEM((gs, cap, dmodel), bf),
            pltpu.VMEM((gs, cap, dmodel), bf),
            pltpu.VMEM((gs, cap, dmodel), bf),
            pltpu.VMEM((cap, dmodel), bf),
            pltpu.VMEM((n_tp, cap, dmodel), bf),
            dma((5,)), dma((3,)), dma((3, CHUNKS)), dma((3, CHUNKS)),
            dma((CHUNKS,)), dma((CHUNKS,)), dma, dma,
            dma((gs, CHUNKS)), dma((gs, CHUNKS)), dma((gs, CHUNKS)), dma((gs, CHUNKS)),
            dma((CHUNKS,)), dma((CHUNKS,)), dma((CHUNKS,)), dma((CHUNKS,)),
        ],
        compiler_params=pltpu.CompilerParams(collective_id=0, has_side_effects=True),
        name="expert_mixture",
    )(
        tokens, norm_gain.reshape(1, dmodel), group_prob.reshape(1, count), route_logits.T,
        expert_ids.T, w_gate, w_up, w_down,
    )


def solution(mesh):
    in_specs = (
        P(("grp", "ep"), None),
        P(),
        P(("grp", "ep")),
        P(("grp", "ep"), None),
        P(("grp", "ep"), None),
        P("ep", None, "tp"),
        P("ep", None, "tp"),
        P("ep", "tp", None),
    )
    out_specs = P(("grp", "ep"), None)
    return jax.shard_map(shards, mesh=mesh, in_specs=in_specs, out_specs=out_specs, check_vma=False)
```

time: 22.2 us -> 21.6 us (0.973)
  Pallas kernels: 21.4 us -> 20.8 us
    pallas_call x1, Pallas kernels: 21.4 us -> 20.8 us  [shards(): pl.pallas_call(functools.partial(kernel, width, n_tp), out_shape=pltpu.VM...]
where the time goes in v1:
time: 21.6 us; the launch traced here: 21.4 us
  Pallas kernels  20.8 us (96%)
  local copies, waits for them, and re-layouts  0.66 us (3%)
    pallas_call x1, Pallas kernels, shards(): pl.pallas_call(functools.partial(kernel, width, n_tp), out_shape=pltpu.VM...  20.8 us
    unnamed x1, local copies, waits for them, and re-layouts  0.66 us

profile of v1, /device:TPU:0, one launch (start us, length us, event | category | flops | bytes accessed | tf_op | source)
XLA Modules:
  0.0 21.4 jit_solution(11126106012987156984)
XLA Ops:
  0.0 20.8 %expert_mixture.1 = bf16[32,2048]{1,0:T(8,128)(2,1)S(1)} custom-call(bf16[32,2048]{1,0:T(8,128)(2,1)} %tok_hbm.1, f32[1,2048]{1,0:T(1,128)} %bitcast.4, f32[1,32]{1,0:T(1,128)} %bitcast.7, f32[4,32]{1,0:T(4,128)} %bitcast.5, s32[4,32]{1,0:T(4,128)} %bitcast.6, bf16[1,2048,256]{2,1,0:T(8,128)(2,1)} %wg_hbm.1, bf16[1,2048,256]{2,1,0:T(8,128)(2,1)} %wu_hbm.1, ...), custom_call_target="tpu_custom_call" | custom-call | tf_op jit(solution)/shard_map/expert_mixture/pallas_call | solution.py:282
  20.8 0.7 %copy.10 = bf16[32,2048]{1,0:T(8,128)(2,1)} copy(bf16[32,2048]{1,0:T(8,128)(2,1)S(1)} %expert_mixture.1) | data formatting | bytes 262144

commit v2 on v1

--- a/solution.py
+++ b/solution.py
@@ -9,6 +9,7 @@
 
 GROUPS = 2
 CHUNKS = 4
+FIRST = 1
 MESH = pl.DeviceIdType.MESH
 
 
@@ -16,7 +17,7 @@
     width, n_tp,
     tok_hbm, gain_hbm, prob_hbm, logit_hbm, ids_hbm, wg_hbm, wu_hbm, wd_hbm,
     out_ref,
-    tok, gain, prob, logit, ids, wg, wu, wd, send, wsend, wroot, x, outs, back, red, mixed,
+    tok, gain, prob, logit, ids, wi, wd, send, wsend, wroot, x, outs, back, red, mixed,
     in_sem, wl_sem, ws_sem, wr_sem, xs_sem, xr_sem, vs_sem, vr_sem,
     ds_sem, dr_sem, bs_sem, br_sem, cs_sem, cr_sem, ms_sem, mr_sem,
 ):
@@ -35,7 +36,9 @@
     own = q != n_tp - 1
     group = (block + q) % GROUPS
     cw = dmodel // CHUNKS
+    ff = wi.shape[3]
     f32, bf = jnp.float32, jnp.bfloat16
+    batches = [(0, FIRST), (FIRST, gs)]
 
     def cols(c):
         return pl.ds(c * cw, cw)
@@ -57,9 +60,9 @@
     ]
     for c in smalls:
         c.start()
-    weights = [(wg_hbm, wg), (wu_hbm, wu), (wd_hbm, wd)]
     loads = [
-        pltpu.make_async_copy(src.at[0], dst.at[q], wl_sem.at[i]) for i, (src, dst) in enumerate(weights)
+        pltpu.make_async_copy(src.at[0], dst, wl_sem.at[i])
+        for i, (src, dst) in enumerate([(wg_hbm, wi.at[0, q]), (wu_hbm, wi.at[1, q]), (wd_hbm, wd.at[q])])
     ]
     for c in loads:
         c.start()
@@ -101,17 +104,16 @@
 
     @pl.when(own)
     def _():
-        x[0] = rows
+        x[local] = rows
 
     pl.semaphore_wait(barrier, jnp.where(cross, gs + 1, gs))
 
     def across(c):
-        return remote(send.at[:, cols(c)], x.at[0, :, cols(c)], xs_sem.at[c], xr_sem.at[c], ep=partner)
+        return remote(send.at[:, cols(c)], x.at[local, :, cols(c)], xs_sem, xr_sem.at[c], ep=partner)
 
     def spread(j, c):
-        return remote(
-            x.at[0, :, cols(c)], x.at[j, :, cols(c)], ds_sem.at[j, c], dr_sem.at[j, c], ep=peer(j)
-        )
+        part = x.at[local, :, cols(c)]
+        return remote(part, part, ds_sem, dr_sem.at[jnp.where(local < FIRST, 0, 1), c], ep=peer(j))
 
     @pl.when(cross)
     def _():
@@ -124,29 +126,18 @@
             for j in range(1, gs):
                 spread(j, c).start()
 
-    def swap(i, c):
-        ref = weights[i][1]
-        part = ref.at[q, cols(c)] if i < 2 else ref.at[q, :, cols(c)]
-        return remote(part, part, ws_sem.at[i, c], wr_sem.at[i, c], tp=sib)
-
-    def swapped(i, c):
-        ref = weights[i][1]
-        part = ref.at[sib, cols(c)] if i < 2 else ref.at[sib, :, cols(c)]
-        return remote(part, part, ws_sem.at[i, c], wr_sem.at[i, c], tp=sib)
-
-    loads[0].wait()
-    loads[1].wait()
-    for c in range(CHUNKS):
-        for i in range(2):
-            swap(i, c).start()
+    def swap(src, dst, i):
+        return remote(src, dst, ws_sem.at[i], wr_sem.at[i], tp=sib)
+
+    for i in range(2):
+        loads[i].wait()
+        swap(wi.at[i, q], wi.at[i, q], 0).start()
     loads[2].wait()
-    for c in range(CHUNKS):
-        swap(2, c).start()
+    swap(wd.at[q], wd.at[q], 1).start()
 
     expw = jnp.exp(logit[...])
     route = prob[...] * expw / jnp.sum(expw, axis=0, keepdims=True)
-    k_io = lax.broadcasted_iota(jnp.int32, (128, count), 0)
-    expert = jnp.where(k_io < gs, group * gs + lax.rem(k_io + local, gs), -1)
+    expert = lax.broadcasted_iota(jnp.int32, (128, count), 0) + group * gs
     wtok = jnp.zeros((128, count), f32)
     for k in range(topk):
         wtok = wtok + jnp.where(idv[k : k + 1, :] == expert, route[k : k + 1, :], 0.0)
@@ -178,46 +169,73 @@
             for j in range(1, gs):
                 spread(j, c).start()
 
-    gates = [jnp.zeros((gs * cap, wg.shape[2]), f32)] * n_tp
-    ups = [jnp.zeros((gs * cap, wu.shape[2]), f32)] * n_tp
-    for c in range(CHUNKS):
-        for i in range(2):
-            swapped(i, c).wait_recv()
-        for j in range(1, gs):
-            spread(j, c).wait_recv()
-        xc = x[:, :, c * cw : (c + 1) * cw].reshape(gs * cap, cw)
-        for h in range(n_tp):
-            gates[h] = gates[h] + jnp.dot(xc, wg[h, c * cw : (c + 1) * cw], preferred_element_type=f32)
-            ups[h] = ups[h] + jnp.dot(xc, wu[h, c * cw : (c + 1) * cw], preferred_element_type=f32)
-    acts = [((g / (1.0 + jnp.exp(-g))) * u).astype(bf) for g, u in zip(gates, ups)]
-
-    def give(j, c):
+    def landed(b, c):
+        lo, hi = batches[b]
+        inside = (local >= lo) & (local < hi)
+
+        def take(n):
+            part = x.at[pl.ds(lo, n), :, cols(c)]
+            remote(part, part, ds_sem, dr_sem.at[b, c], tp=sib).wait_recv()
+
+        if hi - lo > 1:
+
+            @pl.when(inside)
+            def _():
+                take(hi - lo - 1)
+
+        @pl.when(jnp.logical_not(inside))
+        def _():
+            take(hi - lo)
+
+    def give(r, c):
         return remote(
-            outs.at[j, :, cols(c)], back.at[j, :, cols(c)], bs_sem.at[j, c], br_sem.at[j, c],
-            ep=base + (local + gs - j) % gs,
+            outs.at[r, :, cols(c)], back.at[local, :, cols(c)], bs_sem, br_sem.at[c], ep=base + r
         )
 
-    for c in range(CHUNKS):
-        swapped(2, c).wait_recv()
-        total = jnp.dot(acts[0], wd[0, :, c * cw : (c + 1) * cw], preferred_element_type=f32)
-        for h in range(1, n_tp):
-            total = total + jnp.dot(acts[h], wd[h, :, c * cw : (c + 1) * cw], preferred_element_type=f32)
-        outs[:, :, c * cw : (c + 1) * cw] = total.astype(bf).reshape(gs, cap, cw)
-        for j in range(1, gs):
-            give(j, c).start()
+    for b, (lo, hi) in enumerate(batches):
+        n = (hi - lo) * cap
+        gates = [jnp.zeros((n, ff), f32)] * n_tp
+        ups = [jnp.zeros((n, ff), f32)] * n_tp
+        for c in range(CHUNKS):
+            landed(b, c)
+            if b == 0 and c == 0:
+                swap(wi.at[:, sib], wi.at[:, sib], 0).wait_recv()
+            k = slice(c * cw, (c + 1) * cw)
+            xc = x[lo:hi, :, k].reshape(n, cw)
+            for h in range(n_tp):
+                gates[h] = gates[h] + jnp.dot(xc, wi[0, h, k], preferred_element_type=f32)
+                ups[h] = ups[h] + jnp.dot(xc, wi[1, h, k], preferred_element_type=f32)
+        acts = [((g / (1.0 + jnp.exp(-g))) * u).astype(bf) for g, u in zip(gates, ups)]
+        if b == 0:
+            swap(wd.at[sib], wd.at[sib], 1).wait_recv()
+        for c in range(CHUNKS):
+            k = slice(c * cw, (c + 1) * cw)
+            total = jnp.dot(acts[0], wd[0, :, k], preferred_element_type=f32)
+            for h in range(1, n_tp):
+                total = total + jnp.dot(acts[h], wd[h, :, k], preferred_element_type=f32)
+            outs[lo:hi, :, k] = total.astype(bf).reshape(hi - lo, cap, cw)
+            for r in range(lo, hi):
+
+                @pl.when(local == r)
+                def _():
+                    back[r, :, k] = outs[r, :, k]
+
+                @pl.when(local != r)
+                def _():
+                    give(r, c).start()
 
     def home(c):
         return remote(
-            red.at[:, cols(c)], mixed.at[n_tp - 1, :, cols(c)], cs_sem.at[c], cr_sem.at[c], ep=partner
+            red.at[:, cols(c)], mixed.at[n_tp - 1, :, cols(c)], cs_sem, cr_sem.at[c], ep=partner
         )
 
     def share(c):
         part = mixed.at[q, :, cols(c)]
-        return remote(part, part, ms_sem.at[c], mr_sem.at[c], tp=sib)
+        return remote(part, part, ms_sem, mr_sem.at[c], tp=sib)
 
     def shared(c):
         part = mixed.at[sib, :, cols(c)]
-        return remote(part, part, ms_sem.at[c], mr_sem.at[c], tp=sib)
+        return remote(part, part, ms_sem, mr_sem.at[c], tp=sib)
 
     @pl.when(cross)
     def _():
@@ -225,20 +243,22 @@
 
     wv = wroot[...]
     for c in range(CHUNKS):
-        acc = wv[:, 0:1] * outs[0, :, c * cw : (c + 1) * cw].astype(f32)
+        part = back.at[pl.ds(0, gs - 1), :, cols(c)]
+        remote(part, part, bs_sem, br_sem.at[c], tp=sib).wait_recv()
+        k = slice(c * cw, (c + 1) * cw)
+        acc = wv[:, 0:1] * back[0, :, k].astype(f32)
         for j in range(1, gs):
-            give(j, c).wait_recv()
-            acc = acc + wv[:, j : j + 1] * back[j, :, c * cw : (c + 1) * cw].astype(f32)
+            acc = acc + wv[:, j : j + 1] * back[j, :, k].astype(f32)
         done = acc.astype(bf)
 
         @pl.when(cross)
         def _():
-            red[:, c * cw : (c + 1) * cw] = done
+            red[:, k] = done
             home(c).start()
 
         @pl.when(own)
         def _():
-            mixed[0, :, c * cw : (c + 1) * cw] = done
+            mixed[0, :, k] = done
             share(c).start()
 
     @pl.when(cross)
@@ -249,23 +269,22 @@
 
     for c in range(CHUNKS):
         shared(c).wait_recv()
-        slots = mixed[:, :, c * cw : (c + 1) * cw].reshape(count, cw)
-        out_ref[:, c * cw : (c + 1) * cw] = jnp.dot(unplace, slots, preferred_element_type=f32).astype(bf)
+        k = slice(c * cw, (c + 1) * cw)
+        slots = mixed[:, :, k].reshape(count, cw)
+        out_ref[:, k] = jnp.dot(unplace, slots, preferred_element_type=f32).astype(bf)
 
     @pl.when(cross)
     def _():
         weights_across().wait_send()
-        for c in range(CHUNKS):
-            across(c).wait_send()
-            home(c).wait_send()
-
-    for c in range(CHUNKS):
-        for i in range(3):
-            swap(i, c).wait_send()
-        for j in range(1, gs):
-            spread(j, c).wait_send()
-            give(j, c).wait_send()
-        share(c).wait_send()
+        remote(send, send, xs_sem, xr_sem.at[0], tp=sib).wait_send()
+        remote(red, red, cs_sem, cr_sem.at[0], tp=sib).wait_send()
+
+    swap(wi.at[:, q], wi.at[:, q], 0).wait_send()
+    swap(wd.at[q], wd.at[q], 1).wait_send()
+    most = x.at[pl.ds(0, gs - 1)]
+    remote(most, most, ds_sem, dr_sem.at[0, 0], tp=sib).wait_send()
+    remote(most, most, bs_sem, br_sem.at[0], tp=sib).wait_send()
+    remote(mixed.at[q], mixed.at[q], ms_sem, mr_sem.at[0], tp=sib).wait_send()
 
 
 def shards(tokens, norm_gain, group_prob, route_logits, expert_ids, w_gate, w_up, w_down):
@@ -290,8 +309,7 @@
             pltpu.VMEM((1, count), f32),
             pltpu.VMEM((topk, count), f32),
             pltpu.VMEM((topk, count), jnp.int32),
-            pltpu.VMEM((n_tp, dmodel, ff), bf),
-            pltpu.VMEM((n_tp, dmodel, ff), bf),
+            pltpu.VMEM((2, n_tp, dmodel, ff), bf),
             pltpu.VMEM((n_tp, ff, dmodel), bf),
             pltpu.VMEM((cap, dmodel), bf),
             pltpu.VMEM((cap, 128), f32),
@@ -301,10 +319,10 @@
             pltpu.VMEM((gs, cap, dmodel), bf),
             pltpu.VMEM((cap, dmodel), bf),
             pltpu.VMEM((n_tp, cap, dmodel), bf),
-            dma((5,)), dma((3,)), dma((3, CHUNKS)), dma((3, CHUNKS)),
-            dma((CHUNKS,)), dma((CHUNKS,)), dma, dma,
-            dma((gs, CHUNKS)), dma((gs, CHUNKS)), dma((gs, CHUNKS)), dma((gs, CHUNKS)),
-            dma((CHUNKS,)), dma((CHUNKS,)), dma((CHUNKS,)), dma((CHUNKS,)),
+            dma((5,)), dma((3,)), dma((2,)), dma((2,)),
+            dma, dma((CHUNKS,)), dma, dma,
+            dma, dma((2, CHUNKS)), dma, dma((CHUNKS,)),
+            dma, dma((CHUNKS,)), dma, dma((CHUNKS,)),
         ],
         compiler_params=pltpu.CompilerParams(collective_id=0, has_side_effects=True),
         name="expert_mixture",

time: 21.6 us -> 20.4 us (0.944)
  the two profiles are of different devices: /device:TPU:0 before, /device:TPU:11 now
where the time goes in v2:
time: 20.4 us; the launch traced here: 20.3 us
  Pallas kernels  19.6 us (96%)
  local copies, waits for them, and re-layouts  0.66 us (3%)
    pallas_call x1, Pallas kernels, shards(): pl.pallas_call(functools.partial(kernel, width, n_tp), out_shape=pltpu.VM...  19.6 us
    unnamed x1, local copies, waits for them, and re-layouts  0.66 us

profile of v2, /device:TPU:11, one launch (start us, length us, event | category | flops | bytes accessed | tf_op | source)
XLA Modules:
  0.0 20.3 jit_solution(17385851418673886681)
XLA Ops:
  0.0 19.6 %expert_mixture.1 = bf16[32,2048]{1,0:T(8,128)(2,1)S(1)} custom-call(bf16[32,2048]{1,0:T(8,128)(2,1)} %tok_hbm.1, f32[1,2048]{1,0:T(1,128)} %bitcast.4, f32[1,32]{1,0:T(1,128)} %bitcast.7, f32[4,32]{1,0:T(4,128)} %bitcast.5, s32[4,32]{1,0:T(4,128)} %bitcast.6, bf16[1,2048,256]{2,1,0:T(8,128)(2,1)} %wg_hbm.1, bf16[1,2048,256]{2,1,0:T(8,128)(2,1)} %wu_hbm.1, ...), custom_call_target="tpu_custom_call" | custom-call | tf_op jit(solution)/shard_map/expert_mixture/pallas_call | solution.py:301
  19.6 0.7 %copy.10 = bf16[32,2048]{1,0:T(8,128)(2,1)} copy(bf16[32,2048]{1,0:T(8,128)(2,1)S(1)} %expert_mixture.1) | data formatting | bytes 262144

commit v3 on v2

--- a/solution.py
+++ b/solution.py
@@ -10,6 +10,7 @@
 GROUPS = 2
 CHUNKS = 4
 FIRST = 1
+HOLD = 2
 MESH = pl.DeviceIdType.MESH
 
 
@@ -120,20 +121,30 @@
         for c in range(CHUNKS):
             across(c).start()
 
-    @pl.when(own)
-    def _():
+    def spread_all():
         for c in range(CHUNKS):
             for j in range(1, gs):
                 spread(j, c).start()
 
-    def swap(src, dst, i):
-        return remote(src, dst, ws_sem.at[i], wr_sem.at[i], tp=sib)
-
-    for i in range(2):
-        loads[i].wait()
-        swap(wi.at[i, q], wi.at[i, q], 0).start()
+    @pl.when(own & (block == 0))
+    def _():
+        spread_all()
+
+    def swap_in(h, c):
+        part = wi.at[:, h, cols(c)]
+        return remote(part, part, ws_sem.at[0], wr_sem.at[c], tp=sib)
+
+    def swap_down(h, c):
+        part = wd.at[h, :, cols(c)]
+        return remote(part, part, ws_sem.at[1], wr_sem.at[CHUNKS + c], tp=sib)
+
+    for c in loads[:2]:
+        c.wait()
+    for c in range(CHUNKS):
+        swap_in(q, c).start()
     loads[2].wait()
-    swap(wd.at[q], wd.at[q], 1).start()
+    for c in range(CHUNKS):
+        swap_down(q, c).start()
 
     expw = jnp.exp(logit[...])
     route = prob[...] * expw / jnp.sum(expw, axis=0, keepdims=True)
@@ -162,6 +173,14 @@
     role = jnp.where(gcol == block.astype(f32), 0.0, 1.0)
     unplace = jnp.where(s_io == role * cap + pos_col, 1.0, 0.0).astype(bf)
 
+    late = own & (block != 0)
+
+    @pl.when(late)
+    def _():
+        for c in range(HOLD):
+            swap_in(sib, c).wait_recv()
+        spread_all()
+
     @pl.when(cross)
     def _():
         for c in range(CHUNKS):
@@ -198,22 +217,36 @@
         ups = [jnp.zeros((n, ff), f32)] * n_tp
         for c in range(CHUNKS):
             landed(b, c)
-            if b == 0 and c == 0:
-                swap(wi.at[:, sib], wi.at[:, sib], 0).wait_recv()
+            if b == 0 and c >= HOLD:
+                swap_in(sib, c).wait_recv()
+            elif b == 0:
+
+                @pl.when(jnp.logical_not(late))
+                def _():
+                    swap_in(sib, c).wait_recv()
+
             k = slice(c * cw, (c + 1) * cw)
             xc = x[lo:hi, :, k].reshape(n, cw)
             for h in range(n_tp):
                 gates[h] = gates[h] + jnp.dot(xc, wi[0, h, k], preferred_element_type=f32)
                 ups[h] = ups[h] + jnp.dot(xc, wi[1, h, k], preferred_element_type=f32)
         acts = [((g / (1.0 + jnp.exp(-g))) * u).astype(bf) for g, u in zip(gates, ups)]
-        if b == 0:
-            swap(wd.at[sib], wd.at[sib], 1).wait_recv()
-        for c in range(CHUNKS):
+
+        def down(c):
+            if b == 0:
+                swap_down(sib, c).wait_recv()
             k = slice(c * cw, (c + 1) * cw)
             total = jnp.dot(acts[0], wd[0, :, k], preferred_element_type=f32)
             for h in range(1, n_tp):
                 total = total + jnp.dot(acts[h], wd[h, :, k], preferred_element_type=f32)
-            outs[lo:hi, :, k] = total.astype(bf).reshape(hi - lo, cap, cw)
+            return total.astype(bf).reshape(hi - lo, cap, cw)
+
+        ready = down(0)
+        for c in range(CHUNKS):
+            k = slice(c * cw, (c + 1) * cw)
+            outs[lo:hi, :, k] = ready
+            if c + 1 < CHUNKS:
+                ready = down(c + 1)
             for r in range(lo, hi):
 
                 @pl.when(local == r)
@@ -279,8 +312,9 @@
         remote(send, send, xs_sem, xr_sem.at[0], tp=sib).wait_send()
         remote(red, red, cs_sem, cr_sem.at[0], tp=sib).wait_send()
 
-    swap(wi.at[:, q], wi.at[:, q], 0).wait_send()
-    swap(wd.at[q], wd.at[q], 1).wait_send()
+    half_in, half_down = wi.at[:, q], wd.at[q]
+    remote(half_in, half_in, ws_sem.at[0], wr_sem.at[0], tp=sib).wait_send()
+    remote(half_down, half_down, ws_sem.at[1], wr_sem.at[0], tp=sib).wait_send()
     most = x.at[pl.ds(0, gs - 1)]
     remote(most, most, ds_sem, dr_sem.at[0, 0], tp=sib).wait_send()
     remote(most, most, bs_sem, br_sem.at[0], tp=sib).wait_send()
@@ -319,7 +353,7 @@
             pltpu.VMEM((gs, cap, dmodel), bf),
             pltpu.VMEM((cap, dmodel), bf),
             pltpu.VMEM((n_tp, cap, dmodel), bf),
-            dma((5,)), dma((3,)), dma((2,)), dma((2,)),
+            dma((5,)), dma((3,)), dma((2,)), dma((2 * CHUNKS,)),
             dma, dma((CHUNKS,)), dma, dma,
             dma, dma((2, CHUNKS)), dma, dma((CHUNKS,)),
             dma, dma((CHUNKS,)), dma, dma((CHUNKS,)),

time: 20.4 us -> 18.5 us (0.907)
  the two profiles are of different devices: /device:TPU:11 before, /device:TPU:9 now
where the time goes in v3:
time: 18.5 us; the launch traced here: 18.4 us
  Pallas kernels  17.7 us (96%)
  local copies, waits for them, and re-layouts  0.66 us (4%)
    pallas_call x1, Pallas kernels, shards(): pl.pallas_call(functools.partial(kernel, width, n_tp), out_shape=pltpu.VM...  17.7 us
    unnamed x1, local copies, waits for them, and re-layouts  0.66 us

profile of v3, /device:TPU:9, one launch (start us, length us, event | category | flops | bytes accessed | tf_op | source)
XLA Modules:
  0.0 18.4 jit_solution(10216613738721847193)
XLA Ops:
  0.0 17.7 %expert_mixture.1 = bf16[32,2048]{1,0:T(8,128)(2,1)S(1)} custom-call(bf16[32,2048]{1,0:T(8,128)(2,1)} %tok_hbm.1, f32[1,2048]{1,0:T(1,128)} %bitcast.4, f32[1,32]{1,0:T(1,128)} %bitcast.7, f32[4,32]{1,0:T(4,128)} %bitcast.5, s32[4,32]{1,0:T(4,128)} %bitcast.6, bf16[1,2048,256]{2,1,0:T(8,128)(2,1)} %wg_hbm.1, bf16[1,2048,256]{2,1,0:T(8,128)(2,1)} %wu_hbm.1, ...), custom_call_target="tpu_custom_call" | custom-call | tf_op jit(solution)/shard_map/expert_mixture/pallas_call | solution.py:335
  17.7 0.7 %copy.10 = bf16[32,2048]{1,0:T(8,128)(2,1)} copy(bf16[32,2048]{1,0:T(8,128)(2,1)S(1)} %expert_mixture.1) | data formatting | bytes 262144

commit v4 on v3

--- a/solution.py
+++ b/solution.py
@@ -10,7 +10,7 @@
 GROUPS = 2
 CHUNKS = 4
 FIRST = 1
-HOLD = 2
+HOLD = 3
 MESH = pl.DeviceIdType.MESH
 
 
@@ -18,7 +18,7 @@
     width, n_tp,
     tok_hbm, gain_hbm, prob_hbm, logit_hbm, ids_hbm, wg_hbm, wu_hbm, wd_hbm,
     out_ref,
-    tok, gain, prob, logit, ids, wi, wd, send, wsend, wroot, x, outs, back, red, mixed,
+    tok, gain, prob, logit, ids, wi, wd, send, wsend, wroot, x, outs, back, red, got, mixed,
     in_sem, wl_sem, ws_sem, wr_sem, xs_sem, xr_sem, vs_sem, vr_sem,
     ds_sem, dr_sem, bs_sem, br_sem, cs_sem, cr_sem, ms_sem, mr_sem,
 ):
@@ -33,13 +33,14 @@
     local = e % gs
     base = block * gs
     partner = (e + gs) % width
+    far = gs - 1 - local
     cross = q == n_tp - 1
     own = q != n_tp - 1
     group = (block + q) % GROUPS
     cw = dmodel // CHUNKS
     ff = wi.shape[3]
     f32, bf = jnp.float32, jnp.bfloat16
-    batches = [(0, FIRST), (FIRST, gs)]
+    split = cross & (block != 0)
 
     def cols(c):
         return pl.ds(c * cw, cw)
@@ -114,7 +115,7 @@
 
     def spread(j, c):
         part = x.at[local, :, cols(c)]
-        return remote(part, part, ds_sem, dr_sem.at[jnp.where(local < FIRST, 0, 1), c], ep=peer(j))
+        return remote(part, part, ds_sem, dr_sem.at[jnp.where(split & (local >= FIRST), 1, 0), c], ep=peer(j))
 
     @pl.when(cross)
     def _():
@@ -148,7 +149,9 @@
 
     expw = jnp.exp(logit[...])
     route = prob[...] * expw / jnp.sum(expw, axis=0, keepdims=True)
-    expert = lax.broadcasted_iota(jnp.int32, (128, count), 0) + group * gs
+    k_io = lax.broadcasted_iota(jnp.int32, (128, count), 0)
+    column = jnp.where(k_io < gs - 1, k_io + jnp.where(k_io >= far, 1, 0), far)
+    expert = jnp.where(k_io < gs, column + group * gs, -1)
     wtok = jnp.zeros((128, count), f32)
     for k in range(topk):
         wtok = wtok + jnp.where(idv[k : k + 1, :] == expert, route[k : k + 1, :], 0.0)
@@ -160,14 +163,11 @@
     def weights_across():
         return remote(wsend, wroot, vs_sem, vr_sem, ep=partner)
 
-    @pl.when(cross)
-    def _():
-        wsend[...] = wslot
+    wsend[...] = wslot
+
+    @pl.when(cross)
+    def _():
         weights_across().start()
-
-    @pl.when(own)
-    def _():
-        wroot[...] = wslot
 
     s_io = lax.broadcasted_iota(jnp.int32, (count, count), 1).astype(f32)
     role = jnp.where(gcol == block.astype(f32), 0.0, 1.0)
@@ -188,14 +188,16 @@
             for j in range(1, gs):
                 spread(j, c).start()
 
-    def landed(b, c):
-        lo, hi = batches[b]
+    def landed(b, lo, hi, c):
         inside = (local >= lo) & (local < hi)
 
         def take(n):
             part = x.at[pl.ds(lo, n), :, cols(c)]
             remote(part, part, ds_sem, dr_sem.at[b, c], tp=sib).wait_recv()
 
+        if hi - lo == gs:
+            take(gs - 1)
+            return
         if hi - lo > 1:
 
             @pl.when(inside)
@@ -211,12 +213,18 @@
             outs.at[r, :, cols(c)], back.at[local, :, cols(c)], bs_sem, br_sem.at[c], ep=base + r
         )
 
-    for b, (lo, hi) in enumerate(batches):
+    def direct(r, c):
+        return remote(
+            outs.at[r, :, cols(c)], got.at[1, :, cols(c)], bs_sem, cr_sem.at[c],
+            ep=(base + r + gs) % width,
+        )
+
+    def experts(b, lo, hi):
         n = (hi - lo) * cap
         gates = [jnp.zeros((n, ff), f32)] * n_tp
         ups = [jnp.zeros((n, ff), f32)] * n_tp
         for c in range(CHUNKS):
-            landed(b, c)
+            landed(b, lo, hi, c)
             if b == 0 and c >= HOLD:
                 swap_in(sib, c).wait_recv()
             elif b == 0:
@@ -253,13 +261,26 @@
                 def _():
                     back[r, :, k] = outs[r, :, k]
 
-                @pl.when(local != r)
+                @pl.when((local != r) & (own | (far != r)))
                 def _():
                     give(r, c).start()
 
+                @pl.when(cross & (far == r))
+                def _():
+                    direct(r, c).start()
+
+    @pl.when(split)
+    def _():
+        experts(0, 0, FIRST)
+        experts(1, FIRST, gs)
+
+    @pl.when(jnp.logical_not(split))
+    def _():
+        experts(0, 0, gs)
+
     def home(c):
         return remote(
-            red.at[:, cols(c)], mixed.at[n_tp - 1, :, cols(c)], cs_sem, cr_sem.at[c], ep=partner
+            red.at[:, cols(c)], got.at[0, :, cols(c)], cs_sem, cr_sem.at[c], ep=partner
         )
 
     def share(c):
@@ -274,35 +295,51 @@
     def _():
         weights_across().wait_recv()
 
-    wv = wroot[...]
+    wv = jnp.where(cross, wroot[...], wsend[...])
+    near = [i + jnp.where(i >= far, 1, 0) for i in range(gs - 1)]
     for c in range(CHUNKS):
-        part = back.at[pl.ds(0, gs - 1), :, cols(c)]
-        remote(part, part, bs_sem, br_sem.at[c], tp=sib).wait_recv()
         k = slice(c * cw, (c + 1) * cw)
-        acc = wv[:, 0:1] * back[0, :, k].astype(f32)
-        for j in range(1, gs):
-            acc = acc + wv[:, j : j + 1] * back[j, :, k].astype(f32)
-        done = acc.astype(bf)
+
+        def returned(n):
+            part = back.at[pl.ds(0, n), :, cols(c)]
+            remote(part, part, bs_sem, br_sem.at[c], tp=sib).wait_recv()
 
         @pl.when(cross)
         def _():
-            red[:, k] = done
-            home(c).start()
+            returned(gs - 2)
 
         @pl.when(own)
         def _():
-            mixed[0, :, k] = done
+            returned(gs - 1)
+
+        acc = wv[:, 0:1] * back[near[0], :, k].astype(f32)
+        for i in range(1, gs - 1):
+            acc = acc + wv[:, i : i + 1] * back[near[i], :, k].astype(f32)
+
+        @pl.when(cross)
+        def _():
+            red[:, k] = acc.astype(bf)
+            home(c).start()
+
+        @pl.when(own)
+        def _():
+            last = wv[:, gs - 1 : gs] * back[far, :, k].astype(f32)
+            mixed[0, :, k] = (acc + last).astype(bf)
             share(c).start()
 
     @pl.when(cross)
     def _():
         for c in range(CHUNKS):
-            home(c).wait_recv()
+            k = slice(c * cw, (c + 1) * cw)
+            part = got.at[:, :, cols(c)]
+            remote(part, part, cs_sem, cr_sem.at[c], tp=sib).wait_recv()
+            last = wsend[:, gs - 1 : gs] * got[1, :, k].astype(f32)
+            mixed[n_tp - 1, :, k] = (got[0, :, k].astype(f32) + last).astype(bf)
             share(c).start()
 
     for c in range(CHUNKS):
+        k = slice(c * cw, (c + 1) * cw)
         shared(c).wait_recv()
-        k = slice(c * cw, (c + 1) * cw)
         slots = mixed[:, :, k].reshape(count, cw)
         out_ref[:, k] = jnp.dot(unplace, slots, preferred_element_type=f32).astype(bf)
 
@@ -352,6 +389,7 @@
             pltpu.VMEM((gs, cap, dmodel), bf),
             pltpu.VMEM((gs, cap, dmodel), bf),
             pltpu.VMEM((cap, dmodel), bf),
+            pltpu.VMEM((2, cap, dmodel), bf),
             pltpu.VMEM((n_tp, cap, dmodel), bf),
             dma((5,)), dma((3,)), dma((2,)), dma((2 * CHUNKS,)),
             dma, dma((CHUNKS,)), dma, dma,

time: 18.5 us -> 18.6 us (level)
  the two profiles are of different devices: /device:TPU:9 before, /device:TPU:0 now
where the time goes in v4:
time: 18.6 us; the launch traced here: 18.4 us
  Pallas kernels  17.8 us (96%)
  local copies, waits for them, and re-layouts  0.66 us (4%)
    pallas_call x1, Pallas kernels, shards(): pl.pallas_call(functools.partial(kernel, width, n_tp), out_shape=pltpu.VM...  17.8 us
    unnamed x1, local copies, waits for them, and re-layouts  0.66 us

profile of v4, /device:TPU:0, one launch (start us, length us, event | category | flops | bytes accessed | tf_op | source)
XLA Modules:
  0.0 18.4 jit_solution(11486713756240707326)
XLA Ops:
  0.0 17.8 %expert_mixture.1 = bf16[32,2048]{1,0:T(8,128)(2,1)S(1)} custom-call(bf16[32,2048]{1,0:T(8,128)(2,1)} %tok_hbm.1, f32[1,2048]{1,0:T(1,128)} %bitcast.4, f32[1,32]{1,0:T(1,128)} %bitcast.7, f32[4,32]{1,0:T(4,128)} %bitcast.5, s32[4,32]{1,0:T(4,128)} %bitcast.6, bf16[1,2048,256]{2,1,0:T(8,128)(2,1)} %wg_hbm.1, bf16[1,2048,256]{2,1,0:T(8,128)(2,1)} %wu_hbm.1, ...), custom_call_target="tpu_custom_call" | custom-call | tf_op jit(solution)/shard_map/expert_mixture/pallas_call | solution.py:372
  17.8 0.7 %copy.10 = bf16[32,2048]{1,0:T(8,128)(2,1)} copy(bf16[32,2048]{1,0:T(8,128)(2,1)S(1)} %expert_mixture.1) | data formatting | bytes 262144

commit v5 on v4

--- a/solution.py
+++ b/solution.py
@@ -9,7 +9,7 @@
 
 GROUPS = 2
 CHUNKS = 4
-FIRST = 1
+FIRST = 2
 HOLD = 3
 MESH = pl.DeviceIdType.MESH
 
@@ -20,7 +20,7 @@
     out_ref,
     tok, gain, prob, logit, ids, wi, wd, send, wsend, wroot, x, outs, back, red, got, mixed,
     in_sem, wl_sem, ws_sem, wr_sem, xs_sem, xr_sem, vs_sem, vr_sem,
-    ds_sem, dr_sem, bs_sem, br_sem, cs_sem, cr_sem, ms_sem, mr_sem,
+    ds_sem, dr_sem, bs_sem, br_sem, cs_sem, cr_sem, ms_sem, mr_sem, es_sem,
 ):
     e = lax.axis_index("ep")
     q = lax.axis_index("tp")
@@ -41,6 +41,8 @@
     ff = wi.shape[3]
     f32, bf = jnp.float32, jnp.bfloat16
     split = cross & (block != 0)
+    held = split & (local < 1)
+    end = CHUNKS - 1
 
     def cols(c):
         return pl.ds(c * cw, cw)
@@ -151,23 +153,31 @@
     route = prob[...] * expw / jnp.sum(expw, axis=0, keepdims=True)
     k_io = lax.broadcasted_iota(jnp.int32, (128, count), 0)
     column = jnp.where(k_io < gs - 1, k_io + jnp.where(k_io >= far, 1, 0), far)
-    expert = jnp.where(k_io < gs, column + group * gs, -1)
+    column = jnp.where(k_io < gs, column, -1)
+    within = idv - jnp.where(grow > 0.0, gs, 0)
     wtok = jnp.zeros((128, count), f32)
     for k in range(topk):
-        wtok = wtok + jnp.where(idv[k : k + 1, :] == expert, route[k : k + 1, :], 0.0)
-    wslot = lax.dot_general(
-        place, wtok, (((1,), (1,)), ((), ())),
-        precision=lax.Precision.HIGHEST, preferred_element_type=f32,
-    )
+        wtok = wtok + jnp.where(within[k : k + 1, :] == column, route[k : k + 1, :], 0.0)
+
+    def slots_of(placed):
+        return lax.dot_general(
+            placed, wtok, (((1,), (1,)), ((), ())),
+            precision=lax.Precision.HIGHEST, preferred_element_type=f32,
+        )
 
     def weights_across():
         return remote(wsend, wroot, vs_sem, vr_sem, ep=partner)
 
-    wsend[...] = wslot
+    there = jnp.where((pos_row == r_io) & (grow == (1 - block).astype(f32)), 1.0, 0.0)
+    wsend[...] = slots_of(there)
 
     @pl.when(cross)
     def _():
         weights_across().start()
+
+    @pl.when(own)
+    def _():
+        wroot[...] = slots_of(place)
 
     s_io = lax.broadcasted_iota(jnp.int32, (count, count), 1).astype(f32)
     role = jnp.where(gcol == block.astype(f32), 0.0, 1.0)
@@ -213,11 +223,14 @@
             outs.at[r, :, cols(c)], back.at[local, :, cols(c)], bs_sem, br_sem.at[c], ep=base + r
         )
 
-    def direct(r, c):
-        return remote(
-            outs.at[r, :, cols(c)], got.at[1, :, cols(c)], bs_sem, cr_sem.at[c],
-            ep=(base + r + gs) % width,
-        )
+    def both(src, place, c, sem, to):
+        dst = got.at[place, :, cols(c)]
+        remote(src, dst, sem, cr_sem.at[c], ep=to).start()
+        if c == end:
+            remote(src, dst, es_sem, cr_sem.at[c], ep=to, tp=sib).start()
+
+    def send_direct(r, c):
+        both(outs.at[r, :, cols(c)], 1, c, bs_sem, (base + r + gs) % width)
 
     def experts(b, lo, hi):
         n = (hi - lo) * cap
@@ -265,9 +278,9 @@
                 def _():
                     give(r, c).start()
 
-                @pl.when(cross & (far == r))
+                @pl.when(cross & (far == r) & jnp.logical_not(held))
                 def _():
-                    direct(r, c).start()
+                    send_direct(r, c)
 
     @pl.when(split)
     def _():
@@ -277,11 +290,6 @@
     @pl.when(jnp.logical_not(split))
     def _():
         experts(0, 0, gs)
-
-    def home(c):
-        return remote(
-            red.at[:, cols(c)], got.at[0, :, cols(c)], cs_sem, cr_sem.at[c], ep=partner
-        )
 
     def share(c):
         part = mixed.at[q, :, cols(c)]
@@ -295,7 +303,7 @@
     def _():
         weights_across().wait_recv()
 
-    wv = jnp.where(cross, wroot[...], wsend[...])
+    wv = wroot[...]
     near = [i + jnp.where(i >= far, 1, 0) for i in range(gs - 1)]
     for c in range(CHUNKS):
         k = slice(c * cw, (c + 1) * cw)
@@ -319,7 +327,7 @@
         @pl.when(cross)
         def _():
             red[:, k] = acc.astype(bf)
-            home(c).start()
+            both(red.at[:, cols(c)], 0, c, cs_sem, partner)
 
         @pl.when(own)
         def _():
@@ -327,27 +335,56 @@
             mixed[0, :, k] = (acc + last).astype(bf)
             share(c).start()
 
-    @pl.when(cross)
-    def _():
-        for c in range(CHUNKS):
-            k = slice(c * cw, (c + 1) * cw)
-            part = got.at[:, :, cols(c)]
-            remote(part, part, cs_sem, cr_sem.at[c], tp=sib).wait_recv()
-            last = wsend[:, gs - 1 : gs] * got[1, :, k].astype(f32)
-            mixed[n_tp - 1, :, k] = (got[0, :, k].astype(f32) + last).astype(bf)
-            share(c).start()
-
-    for c in range(CHUNKS):
+    @pl.when(held)
+    def _():
+        for c in range(CHUNKS):
+            send_direct(far, c)
+
+    def arrived(c):
         k = slice(c * cw, (c + 1) * cw)
-        shared(c).wait_recv()
+        part = got.at[:, :, cols(c)]
+        remote(part, part, cs_sem, cr_sem.at[c], tp=sib).wait_recv()
+        last = wsend[:, gs - 1 : gs] * got[1, :, k].astype(f32)
+        mixed[n_tp - 1, :, k] = (got[0, :, k].astype(f32) + last).astype(bf)
+
+    def restore(c):
+        k = slice(c * cw, (c + 1) * cw)
         slots = mixed[:, :, k].reshape(count, cw)
         out_ref[:, k] = jnp.dot(unplace, slots, preferred_element_type=f32).astype(bf)
+
+    @pl.when(cross)
+    def _():
+        for c in range(CHUNKS):
+            arrived(c)
+            if c < end:
+                share(c).start()
+            if c > 0:
+                shared(c - 1).wait_recv()
+                restore(c - 1)
+        shared(end).wait_recv()
+        restore(end)
+
+    @pl.when(own)
+    def _():
+        for c in range(end):
+            shared(c).wait_recv()
+            restore(c)
+        arrived(end)
+        restore(end)
 
     @pl.when(cross)
     def _():
         weights_across().wait_send()
         remote(send, send, xs_sem, xr_sem.at[0], tp=sib).wait_send()
         remote(red, red, cs_sem, cr_sem.at[0], tp=sib).wait_send()
+        twice = got.at[:, :, cols(end)]
+        remote(twice, twice, es_sem, cr_sem.at[0], tp=sib).wait_send()
+        most_mixed = mixed.at[q, :, pl.ds(0, end * cw)]
+        remote(most_mixed, most_mixed, ms_sem, mr_sem.at[0], tp=sib).wait_send()
+
+    @pl.when(own)
+    def _():
+        remote(mixed.at[q], mixed.at[q], ms_sem, mr_sem.at[0], tp=sib).wait_send()
 
     half_in, half_down = wi.at[:, q], wd.at[q]
     remote(half_in, half_in, ws_sem.at[0], wr_sem.at[0], tp=sib).wait_send()
@@ -355,7 +392,6 @@
     most = x.at[pl.ds(0, gs - 1)]
     remote(most, most, ds_sem, dr_sem.at[0, 0], tp=sib).wait_send()
     remote(most, most, bs_sem, br_sem.at[0], tp=sib).wait_send()
-    remote(mixed.at[q], mixed.at[q], ms_sem, mr_sem.at[0], tp=sib).wait_send()
 
 
 def shards(tokens, norm_gain, group_prob, route_logits, expert_ids, w_gate, w_up, w_down):
@@ -394,7 +430,7 @@
             dma((5,)), dma((3,)), dma((2,)), dma((2 * CHUNKS,)),
             dma, dma((CHUNKS,)), dma, dma,
             dma, dma((2, CHUNKS)), dma, dma((CHUNKS,)),
-            dma, dma((CHUNKS,)), dma, dma((CHUNKS,)),
+            dma, dma((CHUNKS,)), dma, dma((CHUNKS,)), dma,
         ],
         compiler_params=pltpu.CompilerParams(collective_id=0, has_side_effects=True),
         name="expert_mixture",

time: 18.6 us -> 18 us (0.968)
  Pallas kernels: 17.8 us -> 17.1 us
    pallas_call x1, Pallas kernels: 17.8 us -> 17.1 us  [shards(): pl.pallas_call(functools.partial(kernel, width, n_tp), out_shape=pltpu.VM...]
where the time goes in v5:
time: 18 us; the launch traced here: 17.8 us
  Pallas kernels  17.1 us (95%)
  local copies, waits for them, and re-layouts  0.66 us (4%)
    pallas_call x1, Pallas kernels, shards(): pl.pallas_call(functools.partial(kernel, width, n_tp), out_shape=pltpu.VM...  17.1 us
    unnamed x1, local copies, waits for them, and re-layouts  0.66 us

profile of v5, /device:TPU:0, one launch (start us, length us, event | category | flops | bytes accessed | tf_op | source)
XLA Modules:
  0.0 17.8 jit_solution(6355304282215224908)
XLA Ops:
  0.0 17.1 %expert_mixture.1 = bf16[32,2048]{1,0:T(8,128)(2,1)S(1)} custom-call(bf16[32,2048]{1,0:T(8,128)(2,1)} %tok_hbm.1, f32[1,2048]{1,0:T(1,128)} %bitcast.4, f32[1,32]{1,0:T(1,128)} %bitcast.7, f32[4,32]{1,0:T(4,128)} %bitcast.5, s32[4,32]{1,0:T(4,128)} %bitcast.6, bf16[1,2048,256]{2,1,0:T(8,128)(2,1)} %wg_hbm.1, bf16[1,2048,256]{2,1,0:T(8,128)(2,1)} %wu_hbm.1, ...), custom_call_target="tpu_custom_call" | custom-call | tf_op jit(solution)/shard_map/expert_mixture/pallas_call | solution.py:408
  17.1 0.7 %copy.10 = bf16[32,2048]{1,0:T(8,128)(2,1)} copy(bf16[32,2048]{1,0:T(8,128)(2,1)S(1)} %expert_mixture.1) | data formatting | bytes 262144

commit v6 on v5

--- a/solution.py
+++ b/solution.py
@@ -19,8 +19,7 @@
     tok_hbm, gain_hbm, prob_hbm, logit_hbm, ids_hbm, wg_hbm, wu_hbm, wd_hbm,
     out_ref,
     tok, gain, prob, logit, ids, wi, wd, send, wsend, wroot, x, outs, back, red, got, mixed,
-    in_sem, wl_sem, ws_sem, wr_sem, xs_sem, xr_sem, vs_sem, vr_sem,
-    ds_sem, dr_sem, bs_sem, br_sem, cs_sem, cr_sem, ms_sem, mr_sem, es_sem,
+    in_sem, wl_sem, out_sem, wr_sem, xr_sem, vr_sem, dr_sem, br_sem, cr_sem, mr_sem,
 ):
     e = lax.axis_index("ep")
     q = lax.axis_index("tp")
@@ -57,15 +56,15 @@
         )
 
     smalls = [
-        pltpu.make_async_copy(src, dst, in_sem.at[i])
-        for i, (src, dst) in enumerate(
-            [(tok_hbm, tok), (gain_hbm, gain), (prob_hbm, prob), (logit_hbm, logit), (ids_hbm, ids)]
-        )
+        pltpu.make_async_copy(src, dst, in_sem)
+        for src, dst in [
+            (tok_hbm, tok), (gain_hbm, gain), (prob_hbm, prob), (logit_hbm, logit), (ids_hbm, ids)
+        ]
     ]
     for c in smalls:
         c.start()
     loads = [
-        pltpu.make_async_copy(src.at[0], dst, wl_sem.at[i])
+        pltpu.make_async_copy(src.at[0], dst, wl_sem.at[i // 2])
         for i, (src, dst) in enumerate([(wg_hbm, wi.at[0, q]), (wu_hbm, wi.at[1, q]), (wd_hbm, wd.at[q])])
     ]
     for c in loads:
@@ -113,11 +112,11 @@
     pl.semaphore_wait(barrier, jnp.where(cross, gs + 1, gs))
 
     def across(c):
-        return remote(send.at[:, cols(c)], x.at[local, :, cols(c)], xs_sem, xr_sem.at[c], ep=partner)
+        return remote(send.at[:, cols(c)], x.at[local, :, cols(c)], out_sem, xr_sem.at[c], ep=partner)
 
     def spread(j, c):
         part = x.at[local, :, cols(c)]
-        return remote(part, part, ds_sem, dr_sem.at[jnp.where(split & (local >= FIRST), 1, 0), c], ep=peer(j))
+        return remote(part, part, out_sem, dr_sem.at[jnp.where(split & (local >= FIRST), CHUNKS, c)], ep=peer(j))
 
     @pl.when(cross)
     def _():
@@ -135,11 +134,11 @@
 
     def swap_in(h, c):
         part = wi.at[:, h, cols(c)]
-        return remote(part, part, ws_sem.at[0], wr_sem.at[c], tp=sib)
+        return remote(part, part, out_sem, wr_sem.at[c], tp=sib)
 
     def swap_down(h, c):
         part = wd.at[h, :, cols(c)]
-        return remote(part, part, ws_sem.at[1], wr_sem.at[CHUNKS + c], tp=sib)
+        return remote(part, part, out_sem, wr_sem.at[CHUNKS + c], tp=sib)
 
     for c in loads[:2]:
         c.wait()
@@ -166,7 +165,7 @@
         )
 
     def weights_across():
-        return remote(wsend, wroot, vs_sem, vr_sem, ep=partner)
+        return remote(wsend, wroot, out_sem, vr_sem, ep=partner)
 
     there = jnp.where((pos_row == r_io) & (grow == (1 - block).astype(f32)), 1.0, 0.0)
     wsend[...] = slots_of(there)
@@ -202,9 +201,12 @@
         inside = (local >= lo) & (local < hi)
 
         def take(n):
-            part = x.at[pl.ds(lo, n), :, cols(c)]
-            remote(part, part, ds_sem, dr_sem.at[b, c], tp=sib).wait_recv()
-
+            part = x.at[pl.ds(lo, n), :, cols(c)] if b == 0 else x.at[pl.ds(lo, n)]
+            sem = dr_sem.at[c if b == 0 else CHUNKS]
+            remote(part, part, out_sem, sem, tp=sib).wait_recv()
+
+        if b > 0 and c > 0:
+            return
         if hi - lo == gs:
             take(gs - 1)
             return
@@ -220,17 +222,17 @@
 
     def give(r, c):
         return remote(
-            outs.at[r, :, cols(c)], back.at[local, :, cols(c)], bs_sem, br_sem.at[c], ep=base + r
+            outs.at[r, :, cols(c)], back.at[local, :, cols(c)], out_sem, br_sem.at[c], ep=base + r
         )
 
     def both(src, place, c, sem, to):
         dst = got.at[place, :, cols(c)]
         remote(src, dst, sem, cr_sem.at[c], ep=to).start()
         if c == end:
-            remote(src, dst, es_sem, cr_sem.at[c], ep=to, tp=sib).start()
+            remote(src, dst, out_sem, cr_sem.at[c], ep=to, tp=sib).start()
 
     def send_direct(r, c):
-        both(outs.at[r, :, cols(c)], 1, c, bs_sem, (base + r + gs) % width)
+        both(outs.at[r, :, cols(c)], 1, c, out_sem, (base + r + gs) % width)
 
     def experts(b, lo, hi):
         n = (hi - lo) * cap
@@ -293,11 +295,11 @@
 
     def share(c):
         part = mixed.at[q, :, cols(c)]
-        return remote(part, part, ms_sem, mr_sem.at[c], tp=sib)
+        return remote(part, part, out_sem, mr_sem.at[c], tp=sib)
 
     def shared(c):
         part = mixed.at[sib, :, cols(c)]
-        return remote(part, part, ms_sem, mr_sem.at[c], tp=sib)
+        return remote(part, part, out_sem, mr_sem.at[c], tp=sib)
 
     @pl.when(cross)
     def _():
@@ -310,7 +312,7 @@
 
         def returned(n):
             part = back.at[pl.ds(0, n), :, cols(c)]
-            remote(part, part, bs_sem, br_sem.at[c], tp=sib).wait_recv()
+            remote(part, part, out_sem, br_sem.at[c], tp=sib).wait_recv()
 
         @pl.when(cross)
         def _():
@@ -327,7 +329,7 @@
         @pl.when(cross)
         def _():
             red[:, k] = acc.astype(bf)
-            both(red.at[:, cols(c)], 0, c, cs_sem, partner)
+            both(red.at[:, cols(c)], 0, c, out_sem, partner)
 
         @pl.when(own)
         def _():
@@ -343,7 +345,7 @@
     def arrived(c):
         k = slice(c * cw, (c + 1) * cw)
         part = got.at[:, :, cols(c)]
-        remote(part, part, cs_sem, cr_sem.at[c], tp=sib).wait_recv()
+        remote(part, part, out_sem, cr_sem.at[c], tp=sib).wait_recv()
         last = wsend[:, gs - 1 : gs] * got[1, :, k].astype(f32)
         mixed[n_tp - 1, :, k] = (got[0, :, k].astype(f32) + last).astype(bf)
 
@@ -375,23 +377,23 @@
     @pl.when(cross)
     def _():
         weights_across().wait_send()
-        remote(send, send, xs_sem, xr_sem.at[0], tp=sib).wait_send()
-        remote(red, red, cs_sem, cr_sem.at[0], tp=sib).wait_send()
+        remote(send, send, out_sem, xr_sem.at[0], tp=sib).wait_send()
+        remote(red, red, out_sem, cr_sem.at[0], tp=sib).wait_send()
         twice = got.at[:, :, cols(end)]
-        remote(twice, twice, es_sem, cr_sem.at[0], tp=sib).wait_send()
+        remote(twice, twice, out_sem, cr_sem.at[0], tp=sib).wait_send()
         most_mixed = mixed.at[q, :, pl.ds(0, end * cw)]
-        remote(most_mixed, most_mixed, ms_sem, mr_sem.at[0], tp=sib).wait_send()
+        remote(most_mixed, most_mixed, out_sem, mr_sem.at[0], tp=sib).wait_send()
 
     @pl.when(own)
     def _():
-        remote(mixed.at[q], mixed.at[q], ms_sem, mr_sem.at[0], tp=sib).wait_send()
+        remote(mixed.at[q], mixed.at[q], out_sem, mr_sem.at[0], tp=sib).wait_send()
 
     half_in, half_down = wi.at[:, q], wd.at[q]
-    remote(half_in, half_in, ws_sem.at[0], wr_sem.at[0], tp=sib).wait_send()
-    remote(half_down, half_down, ws_sem.at[1], wr_sem.at[0], tp=sib).wait_send()
+    remote(half_in, half_in, out_sem, wr_sem.at[0], tp=sib).wait_send()
+    remote(half_down, half_down, out_sem, wr_sem.at[0], tp=sib).wait_send()
     most = x.at[pl.ds(0, gs - 1)]
-    remote(most, most, ds_sem, dr_sem.at[0, 0], tp=sib).wait_send()
-    remote(most, most, bs_sem, br_sem.at[0], tp=sib).wait_send()
+    remote(most, most, out_sem, dr_sem.at[0], tp=sib).wait_send()
+    remote(most, most, out_sem, br_sem.at[0], tp=sib).wait_send()
 
 
 def shards(tokens, norm_gain, group_prob, route_logits, expert_ids, w_gate, w_up, w_down):
@@ -427,10 +429,8 @@
             pltpu.VMEM((cap, dmodel), bf),
             pltpu.VMEM((2, cap, dmodel), bf),
             pltpu.VMEM((n_tp, cap, dmodel), bf),
-            dma((5,)), dma((3,)), dma((2,)), dma((2 * CHUNKS,)),
-            dma, dma((CHUNKS,)), dma, dma,
-            dma, dma((2, CHUNKS)), dma, dma((CHUNKS,)),
-            dma, dma((CHUNKS,)), dma, dma((CHUNKS,)), dma,
+            dma, dma((2,)), dma, dma((2 * CHUNKS,)), dma((CHUNKS,)), dma,
+            dma((CHUNKS + 1,)), dma((CHUNKS,)), dma((CHUNKS,)), dma((CHUNKS,)),
         ],
         compiler_params=pltpu.CompilerParams(collective_id=0, has_side_effects=True),
         name="expert_mixture",

time: 18 us -> 17.9 us (level)
  no operation moved by 1% of the time
where the time goes in v6:
time: 17.9 us; the launch traced here: 17.6 us
  Pallas kernels  17 us (95%)
  local copies, waits for them, and re-layouts  0.66 us (4%)
    pallas_call x1, Pallas kernels, shards(): pl.pallas_call(functools.partial(kernel, width, n_tp), out_shape=pltpu.VM...  17 us
    unnamed x1, local copies, waits for them, and re-layouts  0.66 us

profile of v6, /device:TPU:0, one launch (start us, length us, event | category | flops | bytes accessed | tf_op | source)
XLA Modules:
  0.0 17.6 jit_solution(7119241745225056215)
XLA Ops:
  0.0 17.0 %expert_mixture.1 = bf16[32,2048]{1,0:T(8,128)(2,1)S(1)} custom-call(bf16[32,2048]{1,0:T(8,128)(2,1)} %tok_hbm.1, f32[1,2048]{1,0:T(1,128)} %bitcast.4, f32[1,32]{1,0:T(1,128)} %bitcast.7, f32[4,32]{1,0:T(4,128)} %bitcast.5, s32[4,32]{1,0:T(4,128)} %bitcast.6, bf16[1,2048,256]{2,1,0:T(8,128)(2,1)} %wg_hbm.1, bf16[1,2048,256]{2,1,0:T(8,128)(2,1)} %wu_hbm.1, ...), custom_call_target="tpu_custom_call" | custom-call | tf_op jit(solution)/shard_map/expert_mixture/pallas_call | solution.py:410
  17.0 0.7 %copy.10 = bf16[32,2048]{1,0:T(8,128)(2,1)} copy(bf16[32,2048]{1,0:T(8,128)(2,1)S(1)} %expert_mixture.1) | data formatting | bytes 262144

commit v7 on v6

--- a/solution.py
+++ b/solution.py
@@ -11,6 +11,7 @@
 CHUNKS = 4
 FIRST = 2
 HOLD = 3
+TWICE = 1
 MESH = pl.DeviceIdType.MESH
 
 
@@ -41,7 +42,7 @@
     f32, bf = jnp.float32, jnp.bfloat16
     split = cross & (block != 0)
     held = split & (local < 1)
-    end = CHUNKS - 1
+    end = CHUNKS - TWICE
 
     def cols(c):
         return pl.ds(c * cw, cw)
@@ -125,7 +126,7 @@
 
     def spread_all():
         for c in range(CHUNKS):
-            for j in range(1, gs):
+            for j in [*range(1, gs, 2), *range(2, gs, 2)]:
                 spread(j, c).start()
 
     @pl.when(own & (block == 0))
@@ -194,7 +195,7 @@
     def _():
         for c in range(CHUNKS):
             across(c).wait_recv()
-            for j in range(1, gs):
+            for j in [*range(1, gs, 2), *range(2, gs, 2)]:
                 spread(j, c).start()
 
     def landed(b, lo, hi, c):
@@ -227,8 +228,9 @@
 
     def both(src, place, c, sem, to):
         dst = got.at[place, :, cols(c)]
-        remote(src, dst, sem, cr_sem.at[c], ep=to).start()
-        if c == end:
+        early = place == 1 and c == end
+        remote(src, dst, sem, cr_sem.at[CHUNKS if early else c], ep=to).start()
+        if c >= end and place == 0:
             remote(src, dst, out_sem, cr_sem.at[c], ep=to, tp=sib).start()
 
     def send_direct(r, c):
@@ -342,9 +344,14 @@
         for c in range(CHUNKS):
             send_direct(far, c)
 
+    spot = got.at[1, :, cols(end)]
+
+    def pass_on():
+        return remote(spot, spot, out_sem, cr_sem.at[CHUNKS], tp=sib)
+
     def arrived(c):
         k = slice(c * cw, (c + 1) * cw)
-        part = got.at[:, :, cols(c)]
+        part = got.at[0, :, cols(c)] if c == end else got.at[:, :, cols(c)]
         remote(part, part, out_sem, cr_sem.at[c], tp=sib).wait_recv()
         last = wsend[:, gs - 1 : gs] * got[1, :, k].astype(f32)
         mixed[n_tp - 1, :, k] = (got[0, :, k].astype(f32) + last).astype(bf)
@@ -356,21 +363,28 @@
 
     @pl.when(cross)
     def _():
+        pass_on().wait_recv()
+        pass_on().start()
         for c in range(CHUNKS):
             arrived(c)
             if c < end:
                 share(c).start()
-            if c > 0:
+            if c == end - 1:
+                for d in range(c):
+                    shared(d).wait_recv()
+                    restore(d)
+            if c >= end:
                 shared(c - 1).wait_recv()
                 restore(c - 1)
-        shared(end).wait_recv()
-        restore(end)
+        shared(CHUNKS - 1).wait_recv()
+        restore(CHUNKS - 1)
 
     @pl.when(own)
     def _():
         for c in range(end):
             shared(c).wait_recv()
             restore(c)
+        pass_on().wait_recv()
         arrived(end)
         restore(end)
 
@@ -379,7 +393,7 @@
         weights_across().wait_send()
         remote(send, send, out_sem, xr_sem.at[0], tp=sib).wait_send()
         remote(red, red, out_sem, cr_sem.at[0], tp=sib).wait_send()
-        twice = got.at[:, :, cols(end)]
+        twice = got.at[:, :, pl.ds(end * cw, TWICE * cw)]
         remote(twice, twice, out_sem, cr_sem.at[0], tp=sib).wait_send()
         most_mixed = mixed.at[q, :, pl.ds(0, end * cw)]
         remote(most_mixed, most_mixed, out_sem, mr_sem.at[0], tp=sib).wait_send()
@@ -430,7 +444,7 @@
             pltpu.VMEM((2, cap, dmodel), bf),
             pltpu.VMEM((n_tp, cap, dmodel), bf),
             dma, dma((2,)), dma, dma((2 * CHUNKS,)), dma((CHUNKS,)), dma,
-            dma((CHUNKS + 1,)), dma((CHUNKS,)), dma((CHUNKS,)), dma((CHUNKS,)),
+            dma((CHUNKS + 1,)), dma((CHUNKS,)), dma((CHUNKS + 1,)), dma((CHUNKS,)),
         ],
         compiler_params=pltpu.CompilerParams(collective_id=0, has_side_effects=True),
         name="expert_mixture",

time: 17.9 us -> 17.7 us (0.989)
  no operation moved by 1% of the time
where the time goes in v7:
time: 17.7 us; the launch traced here: 17.6 us
  Pallas kernels  16.9 us (95%)
  local copies, waits for them, and re-layouts  0.66 us (4%)
    pallas_call x1, Pallas kernels, shards(): pl.pallas_call(functools.partial(kernel, width, n_tp), out_shape=pltpu.VM...  16.9 us
    unnamed x1, local copies, waits for them, and re-layouts  0.66 us

profile of v7, /device:TPU:0, one launch (start us, length us, event | category | flops | bytes accessed | tf_op | source)
XLA Modules:
  0.0 17.6 jit_solution(16059671631353621284)
XLA Ops:
  0.0 16.9 %expert_mixture.1 = bf16[32,2048]{1,0:T(8,128)(2,1)S(1)} custom-call(bf16[32,2048]{1,0:T(8,128)(2,1)} %tok_hbm.1, f32[1,2048]{1,0:T(1,128)} %bitcast.4, f32[1,32]{1,0:T(1,128)} %bitcast.7, f32[4,32]{1,0:T(4,128)} %bitcast.5, s32[4,32]{1,0:T(4,128)} %bitcast.6, bf16[1,2048,256]{2,1,0:T(8,128)(2,1)} %wg_hbm.1, bf16[1,2048,256]{2,1,0:T(8,128)(2,1)} %wu_hbm.1, ...), custom_call_target="tpu_custom_call" | custom-call | tf_op jit(solution)/shard_map/expert_mixture/pallas_call | solution.py:424
  16.9 0.7 %copy.10 = bf16[32,2048]{1,0:T(8,128)(2,1)} copy(bf16[32,2048]{1,0:T(8,128)(2,1)S(1)} %expert_mixture.1) | data formatting | bytes 262144

commit v8 on v7

--- a/solution.py
+++ b/solution.py
@@ -20,7 +20,7 @@
     tok_hbm, gain_hbm, prob_hbm, logit_hbm, ids_hbm, wg_hbm, wu_hbm, wd_hbm,
     out_ref,
     tok, gain, prob, logit, ids, wi, wd, send, wsend, wroot, x, outs, back, red, got, mixed,
-    in_sem, wl_sem, out_sem, wr_sem, xr_sem, vr_sem, dr_sem, br_sem, cr_sem, mr_sem,
+    in_sem, wl_sem, out_sem, wr_sem, xr_sem, vr_sem, dr_sem, br_sem, cr_sem, mr_sem, ready_sem, go_sem,
 ):
     e = lax.axis_index("ep")
     q = lax.axis_index("tp")
@@ -41,6 +41,7 @@
     ff = wi.shape[3]
     f32, bf = jnp.float32, jnp.bfloat16
     split = cross & (block != 0)
+    late = own & (block != 0)
     held = split & (local < 1)
     end = CHUNKS - TWICE
 
@@ -77,8 +78,11 @@
     def _():
         pl.semaphore_signal(barrier, inc=1, device_id={"ep": partner}, device_id_type=MESH)
 
-    for j in range(1, gs):
-        pl.semaphore_signal(barrier, inc=1, device_id={"ep": peer(j)}, device_id_type=MESH)
+    @pl.when(jnp.logical_not(late))
+    def _():
+        for j in range(1, gs):
+            pl.semaphore_signal(barrier, inc=1, device_id={"ep": peer(j)}, device_id_type=MESH)
+
     pl.semaphore_signal(barrier, inc=1, device_id={"tp": sib}, device_id_type=MESH)
 
     for c in smalls:
@@ -110,7 +114,7 @@
     def _():
         x[local] = rows
 
-    pl.semaphore_wait(barrier, jnp.where(cross, gs + 1, gs))
+    pl.semaphore_wait(barrier, jnp.where(late, 1, jnp.where(cross, gs + 1, gs)))
 
     def across(c):
         return remote(send.at[:, cols(c)], x.at[local, :, cols(c)], out_sem, xr_sem.at[c], ep=partner)
@@ -123,6 +127,11 @@
     def _():
         for c in range(CHUNKS):
             across(c).start()
+
+    @pl.when(split)
+    def _():
+        for j in range(1, gs):
+            pl.semaphore_signal(ready_sem, inc=1, device_id={"ep": peer(j)}, device_id_type=MESH)
 
     def spread_all():
         for c in range(CHUNKS):
@@ -183,10 +192,9 @@
     role = jnp.where(gcol == block.astype(f32), 0.0, 1.0)
     unplace = jnp.where(s_io == role * cap + pos_col, 1.0, 0.0).astype(bf)
 
-    late = own & (block != 0)
-
     @pl.when(late)
     def _():
+        pl.semaphore_wait(go_sem, 1)
         for c in range(HOLD):
             swap_in(sib, c).wait_recv()
         spread_all()
@@ -197,6 +205,12 @@
             across(c).wait_recv()
             for j in [*range(1, gs, 2), *range(2, gs, 2)]:
                 spread(j, c).start()
+            if c == 0:
+
+                @pl.when(split)
+                def _():
+                    pl.semaphore_wait(ready_sem, gs - 1)
+                    pl.semaphore_signal(go_sem, inc=1, device_id={"tp": sib}, device_id_type=MESH)
 
     def landed(b, lo, hi, c):
         inside = (local >= lo) & (local < hi)
@@ -445,6 +459,7 @@
             pltpu.VMEM((n_tp, cap, dmodel), bf),
             dma, dma((2,)), dma, dma((2 * CHUNKS,)), dma((CHUNKS,)), dma,
             dma((CHUNKS + 1,)), dma((CHUNKS,)), dma((CHUNKS + 1,)), dma((CHUNKS,)),
+            pltpu.SemaphoreType.REGULAR, pltpu.SemaphoreType.REGULAR,
         ],
         compiler_params=pltpu.CompilerParams(collective_id=0, has_side_effects=True),
         name="expert_mixture",

time: 17.7 us -> 17.8 us (level)
  no operation moved by 1% of the time
where the time goes in v8:
time: 17.8 us; the launch traced here: 17.6 us
  Pallas kernels  17 us (96%)
  local copies, waits for them, and re-layouts  0.66 us (4%)
    pallas_call x1, Pallas kernels, shards(): pl.pallas_call(functools.partial(kernel, width, n_tp), out_shape=pltpu.VM...  17 us
    unnamed x1, local copies, waits for them, and re-layouts  0.66 us

profile of v8, /device:TPU:0, one launch (start us, length us, event | category | flops | bytes accessed | tf_op | source)
XLA Modules:
  0.0 17.6 jit_solution(13737202845984794938)
XLA Ops:
  0.0 17.0 %expert_mixture.1 = bf16[32,2048]{1,0:T(8,128)(2,1)S(1)} custom-call(bf16[32,2048]{1,0:T(8,128)(2,1)} %tok_hbm.1, f32[1,2048]{1,0:T(1,128)} %bitcast.4, f32[1,32]{1,0:T(1,128)} %bitcast.7, f32[4,32]{1,0:T(4,128)} %bitcast.5, s32[4,32]{1,0:T(4,128)} %bitcast.6, bf16[1,2048,256]{2,1,0:T(8,128)(2,1)} %wg_hbm.1, bf16[1,2048,256]{2,1,0:T(8,128)(2,1)} %wu_hbm.1, ...), custom_call_target="tpu_custom_call" | custom-call | tf_op jit(solution)/shard_map/expert_mixture/pallas_call | solution.py:438
  17.0 0.7 %copy.10 = bf16[32,2048]{1,0:T(8,128)(2,1)} copy(bf16[32,2048]{1,0:T(8,128)(2,1)S(1)} %expert_mixture.1) | data formatting | bytes 262144

commit v9 on v8

--- a/solution.py
+++ b/solution.py
@@ -370,9 +370,9 @@
         last = wsend[:, gs - 1 : gs] * got[1, :, k].astype(f32)
         mixed[n_tp - 1, :, k] = (got[0, :, k].astype(f32) + last).astype(bf)
 
-    def restore(c):
-        k = slice(c * cw, (c + 1) * cw)
-        slots = mixed[:, :, k].reshape(count, cw)
+    def restore(c, n=1):
+        k = slice(c * cw, (c + n) * cw)
+        slots = mixed[:, :, k].reshape(count, n * cw)
         out_ref[:, k] = jnp.dot(unplace, slots, preferred_element_type=f32).astype(bf)
 
     @pl.when(cross)
@@ -387,20 +387,19 @@
                 for d in range(c):
                     shared(d).wait_recv()
                     restore(d)
-            if c >= end:
-                shared(c - 1).wait_recv()
-                restore(c - 1)
-        shared(CHUNKS - 1).wait_recv()
-        restore(CHUNKS - 1)
+        shared(end - 1).wait_recv()
+        shared(end).wait_recv()
+        restore(end - 1, 2)
 
     @pl.when(own)
     def _():
-        for c in range(end):
+        for c in range(end - 1):
             shared(c).wait_recv()
             restore(c)
+        shared(end - 1).wait_recv()
         pass_on().wait_recv()
         arrived(end)
-        restore(end)
+        restore(end - 1, 2)
 
     @pl.when(cross)
     def _():

time: 17.8 us -> 17.6 us (0.989)
  Pallas kernels: 17 us -> 16.8 us
where the time goes in v9:
time: 17.6 us; the launch traced here: 17.5 us
  Pallas kernels  16.8 us (95%)
  local copies, waits for them, and re-layouts  0.66 us (4%)
    pallas_call x1, Pallas kernels, shards(): pl.pallas_call(functools.partial(kernel, width, n_tp), out_shape=pltpu.VM...  16.8 us
    unnamed x1, local copies, waits for them, and re-layouts  0.66 us

profile of v9, /device:TPU:0, one launch (start us, length us, event | category | flops | bytes accessed | tf_op | source)
XLA Modules:
  0.0 17.5 jit_solution(7111789211163559493)
XLA Ops:
  0.0 16.8 %expert_mixture.1 = bf16[32,2048]{1,0:T(8,128)(2,1)S(1)} custom-call(bf16[32,2048]{1,0:T(8,128)(2,1)} %tok_hbm.1, f32[1,2048]{1,0:T(1,128)} %bitcast.4, f32[1,32]{1,0:T(1,128)} %bitcast.7, f32[4,32]{1,0:T(4,128)} %bitcast.5, s32[4,32]{1,0:T(4,128)} %bitcast.6, bf16[1,2048,256]{2,1,0:T(8,128)(2,1)} %wg_hbm.1, bf16[1,2048,256]{2,1,0:T(8,128)(2,1)} %wu_hbm.1, ...), custom_call_target="tpu_custom_call" | custom-call | tf_op jit(solution)/shard_map/expert_mixture/pallas_call | solution.py:437
  16.8 0.7 %copy.10 = bf16[32,2048]{1,0:T(8,128)(2,1)} copy(bf16[32,2048]{1,0:T(8,128)(2,1)S(1)} %expert_mixture.1) | data formatting | bytes 262144
